TPU v7x, 32 devices: a whole 2x2x4 slice. The times are simulated.
32 devices in a mesh: sp: 8 (over z, y), fs: 2 (over x), tp: 2 (over core).
Axes of the slice: x: 2, y: 2, z: 4, core: 2. Of those that a mesh axis runs over, the one named last changes fastest.
Arguments:
- tokens: bfloat16 [8192, 2048], P(('fs', 'sp', 'tp')), parts along dimension 0, may hold values from -60 to 60
- norm_gain: float32 [2048], replicated, may hold values from 0.1 to 1.9
- pool_in: bfloat16 [2048, 512], P('sp', 'tp'), may hold values from -0.125 to 0.125
- gate_in: bfloat16 [2048, 1024], P('sp', 'tp'), may hold values from -0.125 to 0.125
- value_in: bfloat16 [2048, 1024], P('sp', 'tp'), may hold values from -0.125 to 0.125
- pool_mix: bfloat16 [4, 128, 128], P('tp'), may hold values from -0.5 to 0.5
- averaging_factor: float32 [512], P('tp'), may hold values from 0.25 to 0.75
- conv_taps: float32 [4, 1024], P(None, 'tp'), may hold values from -3 to 3
- rate_mix: bfloat16 [16, 64, 64], P('tp'), may hold values from -0.75 to 0.75
- input_mix: bfloat16 [16, 64, 64], P('tp'), may hold values from -0.75 to 0.75
- log_rate: float32 [1024], P('tp'), may hold values from 1.5 to 16
- decay_shift: float32 [32, 4096], P(('fs', 'tp'), 'sp'), parts along dimension 0, may hold values from -1.1 to 0
- initial_state: float32 [2048], P(('fs', 'tp')), parts along dimension 0, may hold values from -6 to 6
- out_pool: bfloat16 [2048, 512], P('sp', 'tp'), may hold values from -0.15625 to 0.15625
- out_rnn: bfloat16 [2048, 1024], P('sp', 'tp'), may hold values from -0.15625 to 0.15625
Outputs:
- mixed: bfloat16 [8192, 2048], P(('fs', 'sp', 'tp')), parts along dimension 0
There are 2 independent parts, one for each index of `fs`. A program takes and returns all parts, laid end to end along the dimension named above; an argument that names none is the same for every part. Nothing has to cross between parts.
All inputs are finite; a program needn't handle non-finite values.
Results may differ from a plain program's by a relative error of at most 0.012.
Values may be sent and summed in bfloat16 or wider, within the bound.
No kernel may reach another device: no remote copies, remote signals or barrier semaphores. Data moves between devices by JAX's collectives and lax.ppermute only.
A program may use at most 64 MiB of HBM per device.

v0:
```python
import jax
import jax.numpy as jnp
from jax import lax
from jax.sharding import PartitionSpec as P

GROUP_WIDTH = 128
HEAD_DIM = 64
TAPS = 4
REACH = 16


epsilon = 1e-06
sharpness = 8.0


def from_behind(value, axis, steps):
    count = lax.axis_size(axis)
    first, last = (max(0, -steps), min(count, count - steps))
    return lax.ppermute(value, axis, [(source, source + steps) for source in range(first, last)])


def carried_in(array, axis, combine, identity):
    count, index = (lax.axis_size(axis), lax.axis_index(axis))
    everything = jax.tree.map(lambda part: lax.all_gather(part, axis), array)
    start = jax.tree.map(
        lambda part, zero: jnp.broadcast_to(jnp.asarray(zero, part.dtype), part.shape),
        array,
        identity,
    )

    def hop(k, before):
        reached = k < index
        new = combine(before, jax.tree.map(lambda part: part[k], everything))
        return jax.tree.map(lambda a, b: jnp.where(reached, a, b), new, before)

    return lax.fori_loop(0, count, hop, start)


def chain_pairs(first_pair, second_pair):
    return (first_pair[0] * second_pair[0], second_pair[0] * first_pair[1] + second_pair[1])


def right_product(left_rows, weight_rows):
    return lax.dot_general(
        left_rows, weight_rows, (((1,), (1,)), ((), ())), preferred_element_type=jnp.float32
    )


def shards(
    tokens,
    norm_gain,
    pool_in,
    gate_in,
    value_in,
    pool_mix,
    averaging_factor,
    conv_taps,
    rate_mix,
    input_mix,
    log_rate,
    decay_shift,
    initial_state,
    out_pool,
    out_rnn,
):
    tp_index = lax.axis_index("tp")
    sp_index = lax.axis_index("sp")
    gathered = (
        lax.all_gather(pool_in, "sp", axis=0, tiled=True),
        lax.all_gather(gate_in, "sp", axis=0, tiled=True),
        lax.all_gather(value_in, "sp", axis=0, tiled=True),
        lax.all_gather(out_pool, "sp", axis=0, tiled=True),
        lax.all_gather(out_rnn, "sp", axis=0, tiled=True),
    )
    pool_weight, gate_weight, value_weight, averaging_exit_matrix, out_rnn_weight = gathered
    pool_width = pool_weight.shape[1]
    rnn_width = gate_weight.shape[1]
    widened = lax.all_gather(tokens, "tp", axis=0, tiled=True).astype(jnp.float32)
    scaling = lax.rsqrt(jnp.mean(widened * widened, axis=1, keepdims=True) + epsilon)
    normed = (widened * scaling * norm_gain[None, :]).astype(jnp.bfloat16)
    outputs = [
        jnp.dot(normed, matrix, preferred_element_type=jnp.float32).astype(jnp.bfloat16)
        for matrix in (pool_weight, gate_weight, value_weight)
    ]
    projected = jnp.concatenate(outputs, axis=1)
    block_rows = projected.shape[0]
    pool_pre = projected[:, :pool_width]
    gate_pre = projected[:, pool_width : pool_width + rnn_width]
    value_pre = projected[:, pool_width + rnn_width :]
    edge_rows = jnp.concatenate(
        [pool_pre[block_rows - REACH :], value_pre[block_rows - REACH :]], axis=1
    )
    earlier_rows = from_behind(edge_rows, "sp", 1)
    pool_values = pool_pre.astype(jnp.float32)
    pool_padded = jnp.concatenate([earlier_rows[:, :pool_width], pool_pre], axis=0).astype(
        jnp.float32
    )
    value_padded = jnp.concatenate([earlier_rows[:, pool_width:], value_pre], axis=0).astype(
        jnp.float32
    )
    groups_here = pool_width // GROUP_WIDTH
    group_index = tp_index * groups_here + jnp.arange(pool_width, dtype=jnp.int32) // GROUP_WIDTH
    window = jnp.left_shift(jnp.int32(2), group_index)
    positions = sp_index * block_rows + jnp.arange(block_rows, dtype=jnp.int32)
    window_sum = jnp.zeros((block_rows, pool_width), jnp.float32)
    for steps_back in range(REACH):
        lagged = pool_padded[REACH - steps_back : REACH - steps_back + block_rows]
        window_sum = window_sum + jnp.where(steps_back < window[None, :], lagged, 0.0)
    counts = jnp.minimum(positions[:, None] + 1, window[None, :]).astype(jnp.float32)
    pooled = (window_sum / counts - pool_values).astype(jnp.bfloat16)
    grouped = pooled.reshape(block_rows, groups_here, GROUP_WIDTH)
    mixed_groups = jnp.einsum("tgc,gcd->tgd", grouped, pool_mix, preferred_element_type=jnp.float32)
    pool_out = (mixed_groups.reshape(block_rows, pool_width) * averaging_factor[None, :]).astype(
        jnp.bfloat16
    )
    start_row = REACH - TAPS + 1
    convolved = conv_taps[0][None, :] * value_padded[start_row : start_row + block_rows]
    for tap_index in range(1, TAPS):
        convolved = (
            convolved
            + conv_taps[tap_index][None, :]
            * value_padded[start_row + tap_index : start_row + tap_index + block_rows]
        )
    conv_out = convolved.astype(jnp.bfloat16)
    heads_here = rnn_width // HEAD_DIM
    both_mixes = jnp.concatenate([rate_mix, input_mix], axis=2)
    gate_terms = jnp.einsum(
        "thc,hcd->thd",
        conv_out.reshape(block_rows, heads_here, HEAD_DIM),
        both_mixes,
        preferred_element_type=jnp.float32,
    )
    rate_gate = jax.nn.sigmoid(gate_terms[:, :, :HEAD_DIM]).reshape(block_rows, rnn_width)
    input_gate = jax.nn.sigmoid(gate_terms[:, :, HEAD_DIM:]).reshape(block_rows, rnn_width)
    shifts = jnp.broadcast_to(
        jnp.transpose(decay_shift)[:, :, None], (block_rows, heads_here, HEAD_DIM)
    ).reshape(block_rows, rnn_width)
    log_decay = -sharpness * rate_gate * jax.nn.softplus(-log_rate)[None, :] + shifts
    decays = jnp.exp(log_decay)
    drives = jnp.sqrt(-jnp.expm1(2.0 * log_decay)) * input_gate * conv_out.astype(jnp.float32)
    cumulative, local_state = lax.associative_scan(chain_pairs, (decays, drives), axis=0)
    identity = (jnp.ones((rnn_width,), jnp.float32), jnp.zeros((rnn_width,), jnp.float32))
    prior_decay, prior_state = carried_in(
        (cumulative[block_rows - 1], local_state[block_rows - 1]), "sp", chain_pairs, identity
    )
    carried = prior_decay * initial_state + prior_state
    hidden_state = local_state + cumulative * carried[None, :]
    rnn_out = (jax.nn.gelu(gate_pre.astype(jnp.float32), approximate=True) * hidden_state).astype(
        jnp.bfloat16
    )
    return lax.psum_scatter(
        right_product(pool_out, averaging_exit_matrix) + right_product(rnn_out, out_rnn_weight),
        "tp",
        scatter_dimension=0,
        tiled=True,
    ).astype(jnp.bfloat16)


def solution(mesh):
    placed = (
        P(("fs", "sp", "tp"), None),
        P(),
        P("sp", "tp"),
        P("sp", "tp"),
        P("sp", "tp"),
        P("tp", None, None),
        P("tp"),
        P(None, "tp"),
        P("tp", None, None),
        P("tp", None, None),
        P("tp"),
        P(("fs", "tp"), "sp"),
        P(("fs", "tp")),
        P("sp", "tp"),
        P("sp", "tp"),
    )
    return jax.shard_map(
        shards, mesh=mesh, in_specs=placed, out_specs=P(("fs", "sp", "tp"), None), check_vma=False
    )
```

profile of v0, /device:TPU:0, one launch (start us, length us, event | category | flops | bytes accessed | tf_op | source)
XLA Modules:
  0.0 381.2 jit_solution(15395088567445469416)
XLA Ops:
  15.7 6.6 %all-gather.9.cloned.1.call-done = bf16[512,2048]{1,0:T(8,128)(2,1)} async-done(((bf16[256,2048]{1,0:T(8,128)(2,1)}), bf16[512,2048]{1,0:T(8,128)(2,1)}) %all-gather.9.cloned.1.call-update) | async-done | bytes 2097168 | tf_op jit(solution)/shard_map/all_gather | solution.py:78
  24.5 41.4 %all-gather.11.cloned.1.call-done = bf16[2048,256]{1,0:T(8,128)(2,1)} async-done(((bf16[256,256]{1,0:T(8,128)(2,1)}), bf16[2048,256]{1,0:T(8,128)(2,1)}) %all-gather.11.cloned.1.call-update) | async-done | bytes 1048592 | tf_op jit(solution)/shard_map/all_gather | solution.py:69
  68.6 47.2 %all-gather.13.cloned.1.call-done = bf16[2048,512]{1,0:T(8,128)(2,1)} async-done(((bf16[256,512]{1,0:T(8,128)(2,1)}), bf16[2048,512]{1,0:T(8,128)(2,1)}) %all-gather.13.cloned.1.call-update) | async-done | bytes 2097168 | tf_op jit(solution)/shard_map/all_gather | solution.py:71
  115.8 2.9 convolution_convert_fusion.1
  119.5 2.6 collective-permute-start
  135.3 2.6 copy.33
  137.9 4.4 %convert_multiply_fusion.5 = (f32[512,512]{1,0:T(8,128)}, f32[512,512]{1,0:T(8,128)}) fusion(f32[512,512]{1,0:T(8,128)} %copy.33, f32[512,512]{1,0:T(8,128)} %copy.32, f32[512,512]{1,0:T(8,128)} %copy.31, f32[512]{0:T(512)S(1)} %fusion.63, f32[528,512]{1,0:T(8,128)S(1)} %maximum_convert_fusion, f32[512]{0:T(512)S(1)} %bitcast.61, f32[512]{0:T(512)S(1)} %bitcast.63, ...), kind=kLoop, calls=%fused_computation.41 | loop fusion | flops 3932160 | bytes 9447424 | tf_op jit(solution)/shard_map/mul | solution.py:140
  142.2 3.7 slice.389
  146.0 3.6 slice.390
  153.7 2.7 multiply_add_fusion.1
  239.5 3.7 slice.452
  253.7 4.6 %pad.127 = f32[512,512]{1,0:T(8,128)} pad(f32[256,512]{1,0:T(8,128)} %add.492, f32[]{:T(128)} %constant.117.clone.1), padding=1_0_1x0_0_0 | pad | bytes 1572868 | tf_op jit(solution)/shard_map/pad | solution.py:141
  260.0 2.6 pad.142
  266.3 2.7 fusion.20
  269.9 4.6 %pad.126 = f32[512,512]{1,0:T(8,128)} pad(f32[256,512]{1,0:T(8,128)} %pad_maximum_fusion, f32[]{:T(128)} %constant.117.clone.1), padding=0_1_1x0_0_0 | pad | bytes 1572868 | tf_op jit(solution)/shard_map/pad | solution.py:141
  275.2 26.7 %all-gather.1 = f32[8,1,512]{2,1,0:T(1,128)S(1)} all-gather(f32[1,1,512]{2,1,0:T(1,128)S(1)} %add_bitcast_fusion), channel_id=1, replica_groups=mesh['sp'=8,'fs'=2,'tp'=2] {'sp'}, dimensions={0}, use_global_device_ids=true | all-gather | bytes 18432 | tf_op jit(solution)/shard_map/all_gather | solution.py:24
  301.9 4.7 %pad.145 = f32[512,512]{1,0:T(8,128)} pad(f32[256,512]{1,0:T(8,128)} %add.502, f32[]{:T(128)} %constant.117.clone.1), padding=1_0_1x0_0_0 | pad | bytes 1572868 | tf_op jit(solution)/shard_map/pad | solution.py:141
  308.6 4.6 %pad.144 = f32[512,512]{1,0:T(8,128)} pad(f32[256,512]{1,0:T(8,128)} %pad_maximum_fusion.1, f32[]{:T(128)} %constant.117.clone.1), padding=0_1_1x0_0_0 | pad | bytes 1572868 | tf_op jit(solution)/shard_map/pad | solution.py:141
  313.9 26.3 %all-gather = f32[8,1,512]{2,1,0:T(1,128)S(1)} all-gather(f32[1,1,512]{2,1,0:T(1,128)S(1)} %add_bitcast_fusion.1), channel_id=1, replica_groups=mesh['sp'=8,'fs'=2,'tp'=2] {'sp'}, dimensions={0}, use_global_device_ids=true | all-gather | bytes 18432 | tf_op jit(solution)/shard_map/all_gather | solution.py:24
  341.6 7.2 %fusion.46 = f32[2,512,128]{1,2,0:T(8,128)S(1)} fusion(bf16[2,128,128]{2,1,0:T(8,128)(2,1)S(1)} %copy-done, bf16[512,256]{1,0:T(8,128)(2,1)S(1)} %copy-done.8, s32[256]{0:T(256)S(1)} %copy-done.46, s32[512]{0:T(512)S(1)} %copy-done.42, f32[528,256]{1,0:T(8,128)} %maximum_convert_fusion.1, pred[256]{0:T(512)(128)(4,1)S(1)} %copy-done.47, ...), kind=kOutput, calls=%fused_computation.93 | convolution fusion | flops 38404096 | bytes 9250560 | tf_op jit(solution)/shard_map/tgc,gcd->tgd/dot_general | solution.py:112
  349.0 4.0 %fusion.77 = f32[512,2048]{1,0:T(8,128)} fusion(bf16[512,256]{0,1:T(8,128)(2,1)S(1)} %fusion.38, bf16[2048,256]{1,0:T(8,128)(2,1)} %all-gather.15.cloned.1.call-done), kind=kOutput, calls=%fused_computation.191 | convolution fusion | flops 536870912 | bytes 5505024 | tf_op jit(solution)/shard_map/dot_general | solution.py:44
  353.0 9.1 %convolution_add_fusion = f32[512,2048]{1,0:T(8,128)} fusion(f32[512,2048]{1,0:T(8,128)} %fusion.77, bf16[2048,512]{1,0:T(8,128)(2,1)} %all-gather.19.cloned.1.call-done, bf16[2048,512]{1,0:T(8,128)(2,1)} %all-gather.17.cloned.1.call-done, f32[512,512]{1,0:T(8,128)} %pad.144, f32[512,512]{1,0:T(8,128)} %pad.145, f32[512,512]{1,0:T(8,128)} %pad.126, ...), kind=kOutput, calls=%fused_computation.9 | convolution fusion | flops 2156920832 | bytes 18886656 | tf_op jit(solution)/shard_map/dot_general | solution.py:44
  362.2 9.4 %reduce-scatter.2.cloned.1.call-done = f32[256,2048]{1,0:T(8,128)} async-done(((f32[512,2048]{1,0:T(8,128)}), f32[256,2048]{1,0:T(8,128)}) %reduce-scatter.2.cloned.1.call-update) | async-done | bytes 2097168 | tf_op jit(solution)/shard_map/reduce_scatter | solution.py:151
  371.6 2.7 convert_element_type.63
  (306 shorter events, 136.3 us)
Async XLA Ops:
  6.5 335.0 %copy-start = (bf16[2,128,128]{2,1,0:T(8,128)(2,1)S(1)}, bf16[2,128,128]{2,1,0:T(8,128)(2,1)}, u32[]{:S(2)}) copy-start(bf16[2,128,128]{2,1,0:T(8,128)(2,1)} %param.22) | copy-start | bytes 196612
  6.5 59.3 %copy-start.23 = (f32[2048]{0:T(1024)S(1)}, f32[2048]{0:T(1024)}, u32[]{:S(2)}) copy-start(f32[2048]{0:T(1024)} %param.18) | copy-start | bytes 24580
  6.5 15.7 %all-gather.9.cloned.1.call-start = ((), (), s32[]{:S(2)}) async-start(), calls=%async_computation.1 | async-start | bytes 3145728 | tf_op jit(solution)/shard_map/all_gather | solution.py:78
  7.3 58.6 %all-gather.11.cloned.1.call-start = ((), (), s32[]{:S(2)}) async-start(), calls=%async_computation.2 | async-start | bytes 1179648 | tf_op jit(solution)/shard_map/all_gather | solution.py:69
  8.0 107.8 %all-gather.13.cloned.1.call-start = ((), (), s32[]{:S(2)}) async-start(), calls=%async_computation.3 | async-start | bytes 2359296 | tf_op jit(solution)/shard_map/all_gather | solution.py:71
  8.8 340.3 %all-gather.15.cloned.1.call-start = ((), (), s32[]{:S(2)}) async-start(), calls=%async_computation.4 | async-start | bytes 1179648 | tf_op jit(solution)/shard_map/all_gather | solution.py:72
  9.3 343.7 %all-gather.17.cloned.1.call-start = ((), (), s32[]{:S(2)}) async-start(), calls=%async_computation.5 | async-start | bytes 2359296 | tf_op jit(solution)/shard_map/all_gather | solution.py:70
  9.9 343.1 %all-gather.19.cloned.1.call-start = ((), (), s32[]{:S(2)}) async-start(), calls=%async_computation.6 | async-start | bytes 2359296 | tf_op jit(solution)/shard_map/all_gather | solution.py:73
  10.5 361.1 %reduce-scatter.2.cloned.1.call-start = ((), (), s32[]{:S(2)}) async-start(), calls=%async_computation.7 | async-start | bytes 6291456 | tf_op jit(solution)/shard_map/reduce_scatter | solution.py:151
  22.2 43.6 %copy-start.1 = (bf16[512,2048]{1,0:T(8,128)(2,1)S(1)}, bf16[512,2048]{1,0:T(8,128)(2,1)}, u32[]{:S(2)}) copy-start(bf16[512,2048]{1,0:T(8,128)(2,1)} %all-gather.9.cloned.1.call-done) | copy-start | bytes 6291460
  24.5 91.3 %copy-start.25 = (f32[512]{0:T(512)}, f32[512]{0:T(512)S(1)}, u32[]{:S(2)}) copy-start(f32[512]{0:T(512)S(1)} %add_rsqrt_fusion) | copy-start | bytes 6148
  68.6 54.1 %copy-start.20 = (f32[8,512]{1,0:T(8,128)S(1)}, f32[8,512]{1,0:T(8,128)}, u32[]{:S(2)}) copy-start(f32[8,512]{1,0:T(8,128)} %param.28) | copy-start | bytes 49156
  119.5 4.6 %collective-permute-start = (bf16[16,768]{1,0:T(8,128)(2,1)S(1)}, bf16[16,768]{1,0:T(8,128)(2,1)S(1)}, u32[]{:S(2)}, u32[]{:S(2)}) collective-permute-start(bf16[16,768]{1,0:T(8,128)(2,1)S(1)} %pad_maximum_fusion.10), channel_id=1, source_target_pairs={{0,4},{4,8},{8,12},{12,16},{16,20},{20,24},{24,28},{1,5},{5,9},{9,... | collective-permute-start | bytes 73736 | tf_op jit(solution)/shard_map/ppermute | solution.py:19
  269.0 37.6 %copy-start.27 = (f32[1,512]{1,0:T(1,128)S(1)}, f32[1,512]{1,0:T(1,128)}, u32[]{:S(2)}) copy-start(f32[1,512]{1,0:T(1,128)} %slice.527) | copy-start | bytes 6148
  301.9 38.4 %copy-start.8 = (bf16[512,256]{1,0:T(8,128)(2,1)S(1)}, bf16[512,256]{1,0:T(8,128)(2,1)}, u32[]{:S(2)}) copy-start(bf16[512,256]{1,0:T(8,128)(2,1)} %copy-done.7) | copy-start | bytes 786436
  301.9 38.4 %slice-start = ((bf16[16,768]{1,0:T(8,128)(2,1)}), bf16[16,256]{1,0:T(8,128)(2,1)S(1)}, s32[]{:S(2)}) async-start(bf16[16,768]{1,0:T(8,128)(2,1)} %copy-done.17), calls=%async_computation.8 | async-start | bytes 16384 | tf_op jit(solution)/shard_map/slice | solution.py:95
  306.6 34.9 %copy-start.44 = (f32[512]{0:T(512)S(1)}, f32[512]{0:T(512)}, u32[]{:S(2)}) copy-start(f32[512]{0:T(512)} %param.29) | copy-start | bytes 6148
  306.6 35.0 %copy-start.42 = (s32[512]{0:T(512)S(1)}, s32[512]{0:T(512)}, u32[]{:S(2)}) copy-start(s32[512]{0:T(512)} %add_add_fusion) | copy-start | bytes 6148
  306.6 35.0 %copy-start.46 = (s32[256]{0:T(256)S(1)}, s32[256]{0:T(256)}, u32[]{:S(2)}) copy-start(s32[256]{0:T(256)} %fusion.65) | copy-start | bytes 3076
  306.6 35.0 %copy-start.47 = (pred[256]{0:T(512)(128)(4,1)S(1)}, pred[256]{0:T(512)(128)(4,1)}, u32[]{:S(2)}) copy-start(pred[256]{0:T(512)(128)(4,1)} %get-tuple-element.200) | copy-start | bytes 772
  306.6 35.0 %copy-start.48 = (pred[256]{0:T(512)(128)(4,1)S(1)}, pred[256]{0:T(512)(128)(4,1)}, u32[]{:S(2)}) copy-start(pred[256]{0:T(512)(128)(4,1)} %get-tuple-element.201) | copy-start | bytes 772
  306.6 35.0 %copy-start.49 = (pred[256]{0:T(512)(128)(4,1)S(1)}, pred[256]{0:T(512)(128)(4,1)}, u32[]{:S(2)}) copy-start(pred[256]{0:T(512)(128)(4,1)} %get-tuple-element.202) | copy-start | bytes 772
  306.6 35.0 %copy-start.50 = (pred[256]{0:T(512)(128)(4,1)S(1)}, pred[256]{0:T(512)(128)(4,1)}, u32[]{:S(2)}) copy-start(pred[256]{0:T(512)(128)(4,1)} %get-tuple-element.203) | copy-start | bytes 772
  306.6 35.0 %copy-start.51 = (pred[256]{0:T(512)(128)(4,1)S(1)}, pred[256]{0:T(512)(128)(4,1)}, u32[]{:S(2)}) copy-start(pred[256]{0:T(512)(128)(4,1)} %get-tuple-element.204) | copy-start | bytes 772
  (37 other events, 389.2 us)
Sparse Core Ops, SparseCore 0:
  8.9 13.2 all-gather.8
  24.3 41.4 all-gather.10
  68.0 47.7 all-gather.12
  117.8 38.7 all-gather.14
  158.6 47.7 all-gather.16
  208.4 47.6 all-gather.18
  362.3 9.2 reduce-scatter.1
where the time goes:
time: 385 us; the launch traced here: 381 us
  local copies, waits for them, and re-layouts  123 us (32%)
  waiting for transfers between devices  108 us (28%)
  blocking collectives  53 us (14%)
  other arithmetic  52.5 us (14%)
  matrix products  26.8 us (7%)
  between operations  14.5 us (4%)
    slice x60, local copies, waits for them, and re-layouts, shards(): lax.associative_scan(chain_pairs, (decays, drives), axis=0)  87.8 us
    all_gather x2, blocking collectives, carried_in(): everything = jax.tree.map(lambda part: lax.all_gather(part, axis), array)  53 us
    all_gather x1, waiting for transfers between devices, shards(): lax.all_gather(value_in, 'sp', axis=0, tiled=True)  47.2 us
    all_gather x1, waiting for transfers between devices, shards(): lax.all_gather(pool_in, 'sp', axis=0, tiled=True)  41.4 us
    pad x32, local copies, waits for them, and re-layouts, shards(): lax.associative_scan(chain_pairs, (decays, drives), axis=0)  24.2 us
    add x16, other arithmetic, chain_pairs(): second_pair[0] * first_pair[1] + second_pair[1]  17.6 us
    dot_general x2, matrix products, right_product(): lax.dot_general(left_rows, weight_rows, (((1,), (1,)), ((), ())), preferr...  13.1 us
    reduce_scatter x1, waiting for transfers between devices, shards(): lax.psum_scatter(right_product(pool_out, averaging_exit_matrix) + right_p...  9.43 us
  transfers between devices with their start and end apart: 8, of which 4 were waited for; matrix products, arithmetic and copies ran while one was open for 49% of the time, Pallas kernels for 0%

commit v1 on v0

v1 whole, which is shorter than its diff:
```python
import jax
import jax.numpy as jnp
from jax import lax
from jax.experimental import pallas as pl
from jax.experimental.pallas import tpu as pltpu
from jax.sharding import PartitionSpec as P

GROUP_WIDTH = 128
HEAD_DIM = 64
TAPS = 4
REACH = 16


epsilon = 1e-06
sharpness = 8.0


def from_behind(value, axis, steps):
    count = lax.axis_size(axis)
    first, last = (max(0, -steps), min(count, count - steps))
    return lax.ppermute(value, axis, [(source, source + steps) for source in range(first, last)])


def right_product(left_rows, weight_rows):
    return lax.dot_general(
        left_rows, weight_rows, (((1,), (1,)), ((), ())), preferred_element_type=jnp.float32
    )


SEGMENTS = 8


def ring_order(place, count):
    half = count // 2
    return jnp.where(place < half, 2 * place, 2 * (count - 1 - place) + 1)


def ring_place(index, count):
    return jnp.where(index % 2 == 0, index // 2, count - 1 - index // 2)


def ring_gather(block, axis):
    count, index = (lax.axis_size(axis), lax.axis_index(axis))
    half = count // 2
    order = [2 * p if p < half else 2 * (count - 1 - p) + 1 for p in range(count)]
    place = ring_place(index, count)
    onward = [(order[p], order[(p + 1) % count]) for p in range(count)]
    backward = [(order[p], order[(p - 1) % count]) for p in range(count)]
    rows = block.shape[0]
    full = jnp.zeros((rows * count, block.shape[1]), block.dtype)

    def put(full, part, source, offset):
        return lax.dynamic_update_slice(
            full, part, (ring_order(source % count, count) * rows + offset, 0)
        )

    full = put(full, block, place, 0)
    right = left = block
    for step in range(1, half):
        right = lax.ppermute(right, axis, onward)
        left = lax.ppermute(left, axis, backward)
        full = put(full, right, place - step + count, 0)
        full = put(full, left, place + step, 0)
    middle = rows // 2
    right = lax.ppermute(right[:middle], axis, onward)
    left = lax.ppermute(left[middle:], axis, backward)
    full = put(full, right, place - half + count, 0)
    return put(full, left, place + half, middle)


def one_minus_exp(x):
    series = 1.0
    for order in range(8, 1, -1):
        series = 1.0 + x * (1.0 / order) * series
    return jnp.where(x > -0.35, -x * series, 1.0 - jnp.exp(x))


def mixer_kernel(
    where_ref,
    pool_ref,
    value_ref,
    edge_pool_ref,
    edge_value_ref,
    pool_mix_ref,
    factor_ref,
    taps_ref,
    gates_ref,
    rate_ref,
    shift_ref,
    pool_out_ref,
    cum_ref,
    state_ref,
    end_ref,
):
    rows = pool_ref.shape[0]
    groups_here = pool_ref.shape[1] // GROUP_WIDTH
    positions = where_ref[1] * rows + lax.broadcasted_iota(jnp.int32, (rows, GROUP_WIDTH), 0)
    for g in range(groups_here):
        cols = slice(g * GROUP_WIDTH, (g + 1) * GROUP_WIDTH)
        window = jnp.left_shift(2, where_ref[0] * groups_here + g)
        own = pool_ref[:, cols].astype(jnp.float32)
        total = jnp.concatenate([edge_pool_ref[:, cols].astype(jnp.float32), own], axis=0)
        reach = 1
        while reach < REACH:
            total = total + jnp.where(reach < window, pltpu.roll(total, reach, 0), 0.0)
            reach *= 2
        counts = jnp.minimum(positions + 1, window).astype(jnp.float32)
        pooled = (total[REACH:] / counts - own).astype(jnp.bfloat16)
        mixed = jnp.dot(pooled, pool_mix_ref[g], preferred_element_type=jnp.float32)
        pool_out_ref[:, cols] = (mixed * factor_ref[:, cols]).astype(jnp.bfloat16)
    width = 2 * HEAD_DIM
    lanes = lax.broadcasted_iota(jnp.int32, (rows, width), 1)
    for p in range(value_ref.shape[1] // width):
        cols = slice(p * width, (p + 1) * width)
        padded = jnp.concatenate([edge_value_ref[:, cols], value_ref[:, cols]], axis=0).astype(
            jnp.float32
        )
        convolved = taps_ref[TAPS - 1 : TAPS, cols] * padded
        for tap in range(TAPS - 1):
            convolved = convolved + taps_ref[tap : tap + 1, cols] * pltpu.roll(
                padded, TAPS - 1 - tap, 0
            )
        conv_out = convolved[REACH:].astype(jnp.bfloat16)
        terms = jnp.dot(conv_out, gates_ref[p], preferred_element_type=jnp.float32)
        rate_gate = jax.nn.sigmoid(terms[:, :width])
        input_gate = jax.nn.sigmoid(terms[:, width:])
        shifts = jnp.where(
            lanes < HEAD_DIM, shift_ref[:, 2 * p : 2 * p + 1], shift_ref[:, 2 * p + 1 : 2 * p + 2]
        )
        log_decay = rate_gate * rate_ref[:, cols] + shifts
        cum_ref[p] = jnp.exp(log_decay)
        state_ref[p] = (
            jnp.sqrt(one_minus_exp(2.0 * log_decay)) * input_gate * conv_out.astype(jnp.float32)
        )
        length = rows // SEGMENTS

        def advance(t, carry):
            product, state = carry
            at = (p, pl.ds(t, SEGMENTS, stride=length), slice(None))
            decay = cum_ref[at]
            product = product * decay
            state = state * decay + state_ref[at]
            cum_ref[at] = product
            state_ref[at] = state
            return product, state

        start = (jnp.ones((SEGMENTS, width), jnp.float32), jnp.zeros((SEGMENTS, width), jnp.float32))
        product, state = lax.fori_loop(0, length, advance, start, unroll=8)
        end_product, end_state = product[:1], state[:1]
        for s in range(1, SEGMENTS):
            end_state = end_state * product[s : s + 1] + state[s : s + 1]
            end_product = end_product * product[s : s + 1]
        end_ref[0:1, cols] = end_product
        end_ref[1:2, cols] = end_state


def finish_kernel(where_ref, gate_ref, cum_ref, state_ref, ends_ref, initial_ref, out_ref):
    rows = gate_ref.shape[0]
    width = 2 * HEAD_DIM
    carried = initial_ref[...]
    for k in range(ends_ref.shape[0] // 2):
        after = carried * ends_ref[2 * k : 2 * k + 1] + ends_ref[2 * k + 1 : 2 * k + 2]
        carried = jnp.where(k < where_ref[1], after, carried)
    length = rows // SEGMENTS
    for p in range(cum_ref.shape[0]):
        cols = slice(p * width, (p + 1) * width)
        before = carried[:, cols]
        for s in range(SEGMENTS):
            span = slice(s * length, (s + 1) * length)
            hidden = state_ref[p, span] + cum_ref[p, span] * before
            gate = jax.nn.gelu(gate_ref[span, cols].astype(jnp.float32), approximate=True)
            out_ref[span, cols] = (gate * hidden).astype(jnp.bfloat16)
            before = hidden[length - 1 : length]


def shards(
    tokens,
    norm_gain,
    pool_in,
    gate_in,
    value_in,
    pool_mix,
    averaging_factor,
    conv_taps,
    rate_mix,
    input_mix,
    log_rate,
    decay_shift,
    initial_state,
    out_pool,
    out_rnn,
):
    tp_index = lax.axis_index("tp")
    sp_index = lax.axis_index("sp")
    where = jnp.stack([tp_index, sp_index]).astype(jnp.int32)
    weight_in = ring_gather(jnp.concatenate([pool_in, value_in, gate_in], axis=1), "sp")
    weight_out = ring_gather(jnp.concatenate([out_pool, out_rnn], axis=1), "sp")
    pool_width = pool_in.shape[1]
    rnn_width = gate_in.shape[1]
    widened = lax.all_gather(tokens, "tp", axis=0, tiled=True).astype(jnp.float32)
    scaling = lax.rsqrt(jnp.mean(widened * widened, axis=1, keepdims=True) + epsilon)
    normed = (widened * scaling * norm_gain[None, :]).astype(jnp.bfloat16)
    projected = jnp.dot(normed, weight_in, preferred_element_type=jnp.float32).astype(jnp.bfloat16)
    block_rows = projected.shape[0]
    front_width = pool_width + rnn_width
    pool_pre = projected[:, :pool_width]
    value_pre = projected[:, pool_width:front_width]
    gate_pre = projected[:, front_width:]
    earlier_rows = from_behind(projected[block_rows - REACH :, :front_width], "sp", 1)
    pairs = rnn_width // (2 * HEAD_DIM)

    def paired(mix):
        halves = mix.reshape(pairs, 2, HEAD_DIM, HEAD_DIM)
        zero = jnp.zeros_like(halves[:, 0])
        upper = jnp.concatenate([halves[:, 0], zero], axis=2)
        lower = jnp.concatenate([zero, halves[:, 1]], axis=2)
        return jnp.concatenate([upper, lower], axis=1)

    gates = jnp.concatenate([paired(rate_mix), paired(input_mix)], axis=2)
    rate = (-sharpness * jax.nn.softplus(-log_rate))[None, :]
    vmem = pl.BlockSpec(memory_space=pltpu.VMEM)
    smem = pl.BlockSpec(memory_space=pltpu.SMEM)
    pool_out, cumulative, local_state, ends = pl.pallas_call(
        mixer_kernel,
        out_shape=(
            jax.ShapeDtypeStruct((block_rows, pool_width), jnp.bfloat16),
            jax.ShapeDtypeStruct((pairs, block_rows, 2 * HEAD_DIM), jnp.float32),
            jax.ShapeDtypeStruct((pairs, block_rows, 2 * HEAD_DIM), jnp.float32),
            jax.ShapeDtypeStruct((2, rnn_width), jnp.float32),
        ),
        in_specs=[smem] + [vmem] * 10,
        out_specs=(vmem,) * 4,
        name="mixer",
    )(
        where,
        pool_pre,
        value_pre,
        earlier_rows[:, :pool_width],
        earlier_rows[:, pool_width:],
        pool_mix,
        averaging_factor[None, :],
        conv_taps,
        gates,
        rate,
        jnp.transpose(decay_shift),
    )
    all_ends = lax.all_gather(ends, "sp", axis=0, tiled=True)
    rnn_out = pl.pallas_call(
        finish_kernel,
        out_shape=jax.ShapeDtypeStruct((block_rows, rnn_width), jnp.bfloat16),
        in_specs=[smem] + [vmem] * 5,
        out_specs=vmem,
        name="finish",
    )(where, gate_pre, cumulative, local_state, all_ends, initial_state[None, :])
    partial = right_product(jnp.concatenate([pool_out, rnn_out], axis=1), weight_out)
    return lax.psum_scatter(partial, "tp", scatter_dimension=0, tiled=True).astype(jnp.bfloat16)


def solution(mesh):
    placed = (
        P(("fs", "sp", "tp"), None),
        P(),
        P("sp", "tp"),
        P("sp", "tp"),
        P("sp", "tp"),
        P("tp", None, None),
        P("tp"),
        P(None, "tp"),
        P("tp", None, None),
        P("tp", None, None),
        P("tp"),
        P(("fs", "tp"), "sp"),
        P(("fs", "tp")),
        P("sp", "tp"),
        P("sp", "tp"),
    )
    return jax.shard_map(
        shards, mesh=mesh, in_specs=placed, out_specs=P(("fs", "sp", "tp"), None), check_vma=False
    )
```

time: 385 us -> 184 us (0.48)
  local copies, waits for them, and re-layouts: 123 us -> 30.2 us
  waiting for transfers between devices: 108 us -> 57.8 us
  other arithmetic: 52.5 us -> 6.91 us
  blocking collectives: 53 us -> 33.3 us
  starting transfers between devices: 2.89 us -> 20.2 us
  matrix products: 26.8 us -> 10.2 us
  Pallas kernels: 0 us -> 11.2 us
    all_gather x5 -> x0, waiting for transfers between devices: 88.6 us -> none  [the longest x1 47.2 us: shards(): lax.all_gather(value_in, 'sp', axis=0, tiled=True)]
    slice x63 -> x7, local copies, waits for them, and re-layouts: 87.8 us -> 2.59 us  [the longest x1 1.06 us: shards(): value_pre = projected[:, pool_width:front_width]]
    ppermute x0 -> x16, waiting for transfers between devices: none -> 46.3 us  [the longest x6 42.1 us: ring_gather(): right = lax.ppermute(right, axis, onward)]
    pad x32 -> x0, local copies, waits for them, and re-layouts: 24.2 us -> none  [shards(): lax.associative_scan(chain_pairs, (decays, drives), axis=0)]
    add x33 -> x0, other arithmetic: 22.7 us -> none  [the longest x16 17.6 us: chain_pairs(): second_pair[0] * first_pair[1] + second_pair[1]]
    all_gather x2 -> x1, blocking collectives: 53 us -> 33.3 us  [shards(): all_ends = lax.all_gather(ends, 'sp', axis=0, tiled=True)]
    ppermute x0 -> x16, starting transfers between devices: none -> 17.5 us  [the longest x6 12.2 us: ring_gather(): right = lax.ppermute(right, axis, onward)]
    dynamic_update_slice x0 -> x18, local copies, waits for them, and re-layouts: none -> 15.2 us  [put(): lax.dynamic_update_slice(full, part, (ring_order(source % count, count) *...]
  transfers between devices with their start and end apart: 8 -> 19, of which waited for: 4 -> 9; matrix products, arithmetic and copies ran while one was open for 49% -> 14% of each run, Pallas kernels for 0% -> 0%
where the time goes in v1:
time: 184 us
  waiting for transfers between devices  57.8 us (31%)
  blocking collectives  33.3 us (18%)
  local copies, waits for them, and re-layouts  30.2 us (16%)
  starting transfers between devices  20.2 us (11%)
  between operations  13.6 us (7%)
  Pallas kernels  11.2 us (6%)
  matrix products  10.2 us (6%)
  other arithmetic  6.91 us (4%)
    ppermute x6, waiting for transfers between devices, ring_gather(): right = lax.ppermute(right, axis, onward)  42.1 us
    all_gather x1, blocking collectives, shards(): all_ends = lax.all_gather(ends, 'sp', axis=0, tiled=True)  33.3 us
    dynamic_update_slice x18, local copies, waits for them, and re-layouts, put(): lax.dynamic_update_slice(full, part, (ring_order(source % count, count) *...  15.2 us
    ppermute x6, starting transfers between devices, ring_gather(): right = lax.ppermute(right, axis, onward)  12.2 us
    reduce_scatter x1, waiting for transfers between devices, shards(): lax.psum_scatter(partial, 'tp', scatter_dimension=0, tiled=True)  11.4 us
    pallas_call x1, Pallas kernels, shards(): pl.pallas_call(mixer_kernel, out_shape=(jax.ShapeDtypeStruct((block_rows,...  8.2 us
    unnamed x19, local copies, waits for them, and re-layouts  5.65 us
    dot_general x1, matrix products, shards(): jnp.dot(normed, weight_in, preferred_element_type=jnp.float32)  5.43 us
  transfers between devices with their start and end apart: 19, of which 9 were waited for; matrix products, arithmetic and copies ran while one was open for 14% of the time, Pallas kernels for 0%

profile of v1, /device:TPU:0, one launch (start us, length us, event | category | flops | bytes accessed | tf_op | source)
XLA Modules:
  0.0 183.5 jit_solution(2937612361709726135)
XLA Ops:
  11.4 3.1 %collective-permute-start = (bf16[256,1280]{1,0:T(8,128)(2,1)}, bf16[256,1280]{1,0:T(8,128)(2,1)}, u32[]{:S(2)}, u32[]{:S(2)}) collective-permute-start(bf16[256,1280]{1,0:T(8,128)(2,1)} %constant_dynamic-update-slice_fusion), channel_id=1, source_target_pairs={{0,8},{8,16},{16,24},{24,28},{28,20},{20,12},{12,4},{4,0},{1,9},{9... | collective-permute-start | bytes 1966088 | tf_op jit(solution)/shard_map/ppermute | solution.py:60
  16.4 2.1 %collective-permute-start.9 = (bf16[256,768]{1,0:T(8,128)(2,1)S(1)}, bf16[256,768]{1,0:T(8,128)(2,1)}, u32[]{:S(2)}, u32[]{:S(2)}) collective-permute-start(bf16[256,768]{1,0:T(8,128)(2,1)S(1)} %constant_dynamic-update-slice_fusion.3), channel_id=1, source_target_pairs={{0,8},{8,16},{16,24},{24,28},{28,20},{20,12},{12,4},{4,0},{1,9},{9... | collective-permute-start | bytes 1179656 | tf_op jit(solution)/shard_map/ppermute | solution.py:60
  18.6 2.7 %broadcast_in_dim.17 = bf16[2048,1280]{1,0:T(8,128)(2,1)} broadcast(bf16[]{:T(256)} %constant.126.clone.1), dimensions={} | broadcast | bytes 5242882 | tf_op jit(solution)/shard_map/broadcast_in_dim | solution.py:50
  21.3 2.0 %constant_dynamic-update-slice_fusion.22 = bf16[2048,1280]{1,0:T(8,128)(2,1)} fusion(bf16[2048,1280]{1,0:T(8,128)(2,1)} %broadcast_in_dim.17, bf16[256,1280]{1,0:T(8,128)(2,1)} %constant_dynamic-update-slice_fusion, s32[]{:T(128)S(6)} %select_n.151), kind=kLoop, calls=%fused_computation.58 | loop fusion | bytes 1310724 | tf_op jit(solution)/shard_map/dynamic_update_slice | solution.py:53
  26.4 11.5 %collective-permute-done.9 = bf16[256,768]{1,0:T(8,128)(2,1)} collective-permute-done((bf16[256,768]{1,0:T(8,128)(2,1)S(1)}, bf16[256,768]{1,0:T(8,128)(2,1)}, u32[]{:S(2)}, u32[]{:S(2)}) %collective-permute-start.9) | collective-permute-done | bytes 393248 | tf_op jit(solution)/shard_map/ppermute | solution.py:60
  37.9 1.8 collective-permute-start.11
  42.0 1.9 %collective-permute-start.2 = (bf16[256,1280]{1,0:T(8,128)(2,1)}, bf16[256,1280]{1,0:T(8,128)(2,1)S(1)}, u32[]{:S(2)}, u32[]{:S(2)}) collective-permute-start(bf16[256,1280]{1,0:T(8,128)(2,1)} %collective-permute-done), channel_id=1, source_target_pairs={{0,8},{8,16},{16,24},{24,28},{28,20},{20,12},{12,4},{4,0},{1,9},{9... | collective-permute-start | bytes 1966088 | tf_op jit(solution)/shard_map/ppermute | solution.py:60
  43.9 2.0 %constant_dynamic-update-slice_fusion.21 = bf16[2048,1280]{1,0:T(8,128)(2,1)} fusion(bf16[2048,1280]{1,0:T(8,128)(2,1)} %constant_dynamic-update-slice_fusion.22, bf16[256,1280]{1,0:T(8,128)(2,1)} %collective-permute-done, s32[]{:T(128)S(6)} %select_n.154), kind=kLoop, calls=%fused_computation.57 | loop fusion | bytes 1310724 | tf_op jit(solution)/shard_map/dynamic_update_slice | solution.py:53
  46.1 4.0 %collective-permute-done.11 = bf16[256,768]{1,0:T(8,128)(2,1)S(1)} collective-permute-done((bf16[256,768]{1,0:T(8,128)(2,1)}, bf16[256,768]{1,0:T(8,128)(2,1)S(1)}, u32[]{:S(2)}, u32[]{:S(2)}) %collective-permute-start.11) | collective-permute-done | bytes 393248 | tf_op jit(solution)/shard_map/ppermute | solution.py:60
  50.1 1.8 collective-permute-start.13
  52.1 2.0 %constant_dynamic-update-slice_fusion.20 = bf16[2048,1280]{1,0:T(8,128)(2,1)} fusion(bf16[2048,1280]{1,0:T(8,128)(2,1)} %constant_dynamic-update-slice_fusion.21, bf16[256,1280]{1,0:T(8,128)(2,1)} %collective-permute-done.1, s32[]{:T(128)S(6)} %select_n.157), kind=kLoop, calls=%fused_computation.56 | loop fusion | bytes 1310724 | tf_op jit(solution)/shard_map/dynamic_update_slice | solution.py:53
  54.2 16.7 %collective-permute-done.13 = bf16[256,768]{1,0:T(8,128)(2,1)S(1)} collective-permute-done((bf16[256,768]{1,0:T(8,128)(2,1)S(1)}, bf16[256,768]{1,0:T(8,128)(2,1)S(1)}, u32[]{:S(2)}, u32[]{:S(2)}) %collective-permute-start.13) | collective-permute-done | bytes 393248 | tf_op jit(solution)/shard_map/ppermute | solution.py:60
  77.0 1.7 collective-permute-done.15
  80.3 9.9 %collective-permute-done.4 = bf16[256,1280]{1,0:T(8,128)(2,1)S(1)} collective-permute-done((bf16[256,1280]{1,0:T(8,128)(2,1)S(1)}, bf16[256,1280]{1,0:T(8,128)(2,1)S(1)}, u32[]{:S(2)}, u32[]{:S(2)}) %collective-permute-start.4) | collective-permute-done | bytes 655392 | tf_op jit(solution)/shard_map/ppermute | solution.py:60
  94.8 2.2 %fusion = f32[512]{0:T(512)S(1)} fusion(bf16[512,2048]{1,0:T(8,128)(2,1)} %all-gather.3.cloned.1.call-done), kind=kLoop, calls=%fused_computation.2 | loop fusion | flops 3145216 | bytes 2099200 | tf_op jit(solution)/shard_map/reduce_sum | solution.py:201
  99.7 1.7 constant_dynamic-update-slice_fusion.14
  101.4 5.4 %convolution_convert_fusion = bf16[512,1280]{1,0:T(8,128)(2,1)S(1)} fusion(bf16[2048,1280]{1,0:T(8,128)(2,1)} %constant_dynamic-update-slice_fusion.14, bf16[512,2048]{1,0:T(8,128)(2,1)S(1)} %copy-done, f32[2048]{0:T(1024)S(1)} %copy-done.6, f32[512]{0:T(512)S(1)} %add_rsqrt_fusion), kind=kOutput, calls=%fused_computation.5 | convolution fusion | flops 2689204224 | bytes 8660992 | tf_op jit(solution)/shard_map/dot_general | solution.py:203
  106.9 2.6 %collective-permute-start.8 = (bf16[16,768]{1,0:T(8,128)(2,1)S(1)}, bf16[16,768]{1,0:T(8,128)(2,1)S(1)}, u32[]{:S(2)}, u32[]{:S(2)}) collective-permute-start(bf16[16,768]{1,0:T(8,128)(2,1)S(1)} %slice.60), channel_id=1, source_target_pairs={{0,4},{4,8},{8,12},{12,16},{16,20},{20,24},{24,28},{1,5},{5,9},{9,... | collective-permute-start | bytes 73736 | tf_op jit(solution)/shard_map/ppermute | solution.py:21
  112.5 8.2 %mixer.1 = (bf16[512,256]{1,0:T(8,128)(2,1)}, f32[4,512,128]{2,1,0:T(8,128)}, f32[4,512,128]{2,1,0:T(8,128)}, f32[2,512]{1,0:T(2,128)}) custom-call(s32[2]{0:T(128)} %pad_add_fusion.where_ref, bf16[512,256]{1,0:T(8,128)(2,1)} %slice.58.pool_ref, bf16[512,512]{1,0:T(8,128)(2,1)} %get-tuple-element.13.value_ref, bf16[16,256]{1,0:T(8,128)(2,1)} %slice.61.edge_pool_ref, ...), custom_call_target="tpu_custom_call" | custom-call | tf_op jit(solution)/shard_map/mixer/pallas_call | solution.py:223
  120.7 33.3 %all-gather = f32[8,2,512]{2,1,0:T(2,128)S(1)} all-gather(f32[1,2,512]{2,1,0:T(2,128)} %bitcast.31), channel_id=1, replica_groups=mesh['sp'=8,'fs'=2,'tp'=2] {'sp'}, dimensions={0}, use_global_device_ids=true | all-gather | bytes 36864 | tf_op jit(solution)/shard_map/all_gather | solution.py:247
  154.7 3.0 %finish.1 = bf16[512,512]{1,0:T(8,128)(2,1)} custom-call(s32[2]{0:T(128)} %pad_add_fusion.where_ref, bf16[512,512]{1,0:T(8,128)(2,1)} %get-tuple-element.14.gate_ref, f32[4,512,128]{2,1,0:T(8,128)} %get-tuple-element.10.cum_ref, f32[4,512,128]{2,1,0:T(8,128)} %get-tuple-element.11.state_ref, f32[16,512]{1,0:T(8,128)} %reshape.18.ends_ref, f32[1,512]{1,0:T(1,128)} %bitcast.32), custom_call_target="tpu_custom_call" | custom-call | tf_op jit(solution)/shard_map/finish/pallas_call | solution.py:248
  157.7 4.8 %fusion.6 = f32[512,2048]{1,0:T(8,128)} fusion(bf16[2048,768]{1,0:T(8,128)(2,1)S(1)} %constant_dynamic-update-slice_fusion.5, bf16[512,512]{1,0:T(8,128)(2,1)} %finish.1, bf16[512,256]{1,0:T(8,128)(2,1)S(1)} %copy-done.5), kind=kOutput, calls=%fused_computation.8 | convolution fusion | flops 1612185600 | bytes 8126464 | tf_op jit(solution)/shard_map/dot_general | solution.py:25
  162.5 11.4 %reduce-scatter.2.cloned.1.call-done = f32[256,2048]{1,0:T(8,128)} async-done(((f32[512,2048]{1,0:T(8,128)}), f32[256,2048]{1,0:T(8,128)}) %reduce-scatter.2.cloned.1.call-update) | async-done | bytes 2097168 | tf_op jit(solution)/shard_map/reduce_scatter | solution.py:256
  174.0 2.7 %convert_element_type.15 = bf16[256,2048]{1,0:T(8,128)(2,1)} convert(f32[256,2048]{1,0:T(8,128)} %reduce-scatter.2.cloned.1.call-done) | non-fusion elementwise | flops 524288 | bytes 3145728 | tf_op jit(solution)/shard_map/convert_element_type | solution.py:256
  (78 shorter events, 31.3 us)
Async XLA Ops:
  6.5 88.3 %all-gather.3.cloned.1.call-start = ((), (), s32[]{:S(2)}) async-start(), calls=%async_computation.1 | async-start | bytes 3145728 | tf_op jit(solution)/shard_map/all_gather | solution.py:200
  11.4 30.6 %collective-permute-start = (bf16[256,1280]{1,0:T(8,128)(2,1)}, bf16[256,1280]{1,0:T(8,128)(2,1)}, u32[]{:S(2)}, u32[]{:S(2)}) collective-permute-start(bf16[256,1280]{1,0:T(8,128)(2,1)} %constant_dynamic-update-slice_fusion), channel_id=1, source_target_pairs={{0,8},{8,16},{16,24},{24,28},{28,20},{20,12},{12,4},{4,0},{1,9},{9... | collective-permute-start | bytes 1966088 | tf_op jit(solution)/shard_map/ppermute | solution.py:60
  14.5 31.4 %collective-permute-start.1 = (bf16[256,1280]{1,0:T(8,128)(2,1)}, bf16[256,1280]{1,0:T(8,128)(2,1)}, u32[]{:S(2)}, u32[]{:S(2)}) collective-permute-start(bf16[256,1280]{1,0:T(8,128)(2,1)} %constant_dynamic-update-slice_fusion), channel_id=1, source_target_pairs={{0,4},{8,0},{16,8},{24,16},{28,24},{20,28},{12,20},{4,12},{1,5},{9... | collective-permute-start | bytes 1966088 | tf_op jit(solution)/shard_map/ppermute | solution.py:61
  16.4 21.5 %collective-permute-start.9 = (bf16[256,768]{1,0:T(8,128)(2,1)S(1)}, bf16[256,768]{1,0:T(8,128)(2,1)}, u32[]{:S(2)}, u32[]{:S(2)}) collective-permute-start(bf16[256,768]{1,0:T(8,128)(2,1)S(1)} %constant_dynamic-update-slice_fusion.3), channel_id=1, source_target_pairs={{0,8},{8,16},{16,24},{24,28},{28,20},{20,12},{12,4},{4,0},{1,9},{9... | collective-permute-start | bytes 1179656 | tf_op jit(solution)/shard_map/ppermute | solution.py:60
  18.5 21.2 %collective-permute-start.10 = (bf16[256,768]{1,0:T(8,128)(2,1)S(1)}, bf16[256,768]{1,0:T(8,128)(2,1)}, u32[]{:S(2)}, u32[]{:S(2)}) collective-permute-start(bf16[256,768]{1,0:T(8,128)(2,1)S(1)} %constant_dynamic-update-slice_fusion.3), channel_id=1, source_target_pairs={{0,4},{8,0},{16,8},{24,16},{28,24},{20,28},{12,20},{4,12},{1,5},{9... | collective-permute-start | bytes 1179656 | tf_op jit(solution)/shard_map/ppermute | solution.py:61
  18.5 155.5 %reduce-scatter.2.cloned.1.call-start = ((), (), s32[]{:S(2)}) async-start(), calls=%async_computation.2 | async-start | bytes 6291456 | tf_op jit(solution)/shard_map/reduce_scatter | solution.py:256
  18.6 4.7 %copy-start.4 = (f32[512]{0:T(512)S(1)}, f32[512]{0:T(512)}, u32[]{:S(2)}) copy-start(f32[512]{0:T(512)} %param.25) | copy-start | bytes 6148
  18.6 6.7 %copy-start.3 = (f32[8,512]{1,0:T(8,128)S(1)}, f32[8,512]{1,0:T(8,128)}, u32[]{:S(2)}) copy-start(f32[8,512]{1,0:T(8,128)} %param.26) | copy-start | bytes 49156
  37.9 12.2 %collective-permute-start.11 = (bf16[256,768]{1,0:T(8,128)(2,1)}, bf16[256,768]{1,0:T(8,128)(2,1)S(1)}, u32[]{:S(2)}, u32[]{:S(2)}) collective-permute-start(bf16[256,768]{1,0:T(8,128)(2,1)} %collective-permute-done.9), channel_id=1, source_target_pairs={{0,8},{8,16},{16,24},{24,28},{28,20},{20,12},{12,4},{4,0},{1,9},{9... | collective-permute-start | bytes 1179656 | tf_op jit(solution)/shard_map/ppermute | solution.py:60
  39.7 12.2 %collective-permute-start.12 = (bf16[256,768]{1,0:T(8,128)(2,1)}, bf16[256,768]{1,0:T(8,128)(2,1)S(1)}, u32[]{:S(2)}, u32[]{:S(2)}) collective-permute-start(bf16[256,768]{1,0:T(8,128)(2,1)} %collective-permute-done.10), channel_id=1, source_target_pairs={{0,4},{8,0},{16,8},{24,16},{28,24},{20,28},{12,20},{4,12},{1,5},{9... | collective-permute-start | bytes 1179656 | tf_op jit(solution)/shard_map/ppermute | solution.py:61
  42.0 31.1 %collective-permute-start.2 = (bf16[256,1280]{1,0:T(8,128)(2,1)}, bf16[256,1280]{1,0:T(8,128)(2,1)S(1)}, u32[]{:S(2)}, u32[]{:S(2)}) collective-permute-start(bf16[256,1280]{1,0:T(8,128)(2,1)} %collective-permute-done), channel_id=1, source_target_pairs={{0,8},{8,16},{16,24},{24,28},{28,20},{20,12},{12,4},{4,0},{1,9},{9... | collective-permute-start | bytes 1966088 | tf_op jit(solution)/shard_map/ppermute | solution.py:60
  45.9 28.8 %collective-permute-start.3 = (bf16[256,1280]{1,0:T(8,128)(2,1)}, bf16[256,1280]{1,0:T(8,128)(2,1)S(1)}, u32[]{:S(2)}, u32[]{:S(2)}) collective-permute-start(bf16[256,1280]{1,0:T(8,128)(2,1)} %collective-permute-done.1), channel_id=1, source_target_pairs={{0,4},{8,0},{16,8},{24,16},{28,24},{20,28},{12,20},{4,12},{1,5},{9... | collective-permute-start | bytes 1966088 | tf_op jit(solution)/shard_map/ppermute | solution.py:61
  50.1 20.8 %collective-permute-start.13 = (bf16[256,768]{1,0:T(8,128)(2,1)S(1)}, bf16[256,768]{1,0:T(8,128)(2,1)S(1)}, u32[]{:S(2)}, u32[]{:S(2)}) collective-permute-start(bf16[256,768]{1,0:T(8,128)(2,1)S(1)} %collective-permute-done.11), channel_id=1, source_target_pairs={{0,8},{8,16},{16,24},{24,28},{28,20},{20,12},{12,4},{4,0},{1,9},{9... | collective-permute-start | bytes 1179656 | tf_op jit(solution)/shard_map/ppermute | solution.py:60
  51.9 20.6 %collective-permute-start.14 = (bf16[256,768]{1,0:T(8,128)(2,1)S(1)}, bf16[256,768]{1,0:T(8,128)(2,1)S(1)}, u32[]{:S(2)}, u32[]{:S(2)}) collective-permute-start(bf16[256,768]{1,0:T(8,128)(2,1)S(1)} %collective-permute-done.12), channel_id=1, source_target_pairs={{0,4},{8,0},{16,8},{24,16},{28,24},{20,28},{12,20},{4,12},{1,5},{9... | collective-permute-start | bytes 1179656 | tf_op jit(solution)/shard_map/ppermute | solution.py:61
  70.9 7.8 %collective-permute-start.15 = (bf16[128,768]{1,0:T(8,128)(2,1)S(1)}, bf16[128,768]{1,0:T(8,128)(2,1)S(1)}, u32[]{:S(2)}, u32[]{:S(2)}) collective-permute-start(bf16[128,768]{1,0:T(8,128)(2,1)S(1)} %slice.68), channel_id=1, source_target_pairs={{0,8},{8,16},{16,24},{24,28},{28,20},{20,12},{12,4},{4,0},{1,9},{9... | collective-permute-start | bytes 589832 | tf_op jit(solution)/shard_map/ppermute | solution.py:65
  72.5 7.8 %collective-permute-start.16 = (bf16[128,768]{1,0:T(8,128)(2,1)S(1)}, bf16[128,768]{1,0:T(8,128)(2,1)S(1)}, u32[]{:S(2)}, u32[]{:S(2)}) collective-permute-start(bf16[128,768]{1,0:T(8,128)(2,1)S(1)} %slice.69), channel_id=1, source_target_pairs={{0,4},{8,0},{16,8},{24,16},{28,24},{20,28},{12,20},{4,12},{1,5},{9... | collective-permute-start | bytes 589832 | tf_op jit(solution)/shard_map/ppermute | solution.py:66
  73.1 17.1 %collective-permute-start.4 = (bf16[256,1280]{1,0:T(8,128)(2,1)S(1)}, bf16[256,1280]{1,0:T(8,128)(2,1)S(1)}, u32[]{:S(2)}, u32[]{:S(2)}) collective-permute-start(bf16[256,1280]{1,0:T(8,128)(2,1)S(1)} %collective-permute-done.2), channel_id=1, source_target_pairs={{0,8},{8,16},{16,24},{24,28},{28,20},{20,12},{12,4},{4,0},{1,9},{9... | collective-permute-start | bytes 1966088 | tf_op jit(solution)/shard_map/ppermute | solution.py:60
  74.7 16.9 %collective-permute-start.5 = (bf16[256,1280]{1,0:T(8,128)(2,1)S(1)}, bf16[256,1280]{1,0:T(8,128)(2,1)S(1)}, u32[]{:S(2)}, u32[]{:S(2)}) collective-permute-start(bf16[256,1280]{1,0:T(8,128)(2,1)S(1)} %collective-permute-done.3), channel_id=1, source_target_pairs={{0,4},{8,0},{16,8},{24,16},{28,24},{20,28},{12,20},{4,12},{1,5},{9... | collective-permute-start | bytes 1966088 | tf_op jit(solution)/shard_map/ppermute | solution.py:61
  90.2 7.3 %collective-permute-start.6 = (bf16[128,1280]{1,0:T(8,128)(2,1)S(1)}, bf16[128,1280]{1,0:T(8,128)(2,1)}, u32[]{:S(2)}, u32[]{:S(2)}) collective-permute-start(bf16[128,1280]{1,0:T(8,128)(2,1)S(1)} %slice.56), channel_id=1, source_target_pairs={{0,8},{8,16},{16,24},{24,28},{28,20},{20,12},{12,4},{4,0},{1,9},{9... | collective-permute-start | bytes 983048 | tf_op jit(solution)/shard_map/ppermute | solution.py:65
  92.3 9.1 %copy-start.6 = (f32[2048]{0:T(1024)S(1)}, f32[2048]{0:T(1024)}, u32[]{:S(2)}) copy-start(f32[2048]{0:T(1024)} %param.16) | copy-start | bytes 24580
  92.3 7.4 %collective-permute-start.7 = (bf16[128,1280]{1,0:T(8,128)(2,1)}, bf16[128,1280]{1,0:T(8,128)(2,1)}, u32[]{:S(2)}, u32[]{:S(2)}) collective-permute-start(bf16[128,1280]{1,0:T(8,128)(2,1)} %slice.57), channel_id=1, source_target_pairs={{0,4},{8,0},{16,8},{24,16},{28,24},{20,28},{12,20},{4,12},{1,5},{9... | collective-permute-start | bytes 983048 | tf_op jit(solution)/shard_map/ppermute | solution.py:66
  94.8 6.6 %copy-start = (bf16[512,2048]{1,0:T(8,128)(2,1)S(1)}, bf16[512,2048]{1,0:T(8,128)(2,1)}, u32[]{:S(2)}) copy-start(bf16[512,2048]{1,0:T(8,128)(2,1)} %all-gather.3.cloned.1.call-done) | copy-start | bytes 6291460
  106.9 4.4 %collective-permute-start.8 = (bf16[16,768]{1,0:T(8,128)(2,1)S(1)}, bf16[16,768]{1,0:T(8,128)(2,1)S(1)}, u32[]{:S(2)}, u32[]{:S(2)}) collective-permute-start(bf16[16,768]{1,0:T(8,128)(2,1)S(1)} %slice.60), channel_id=1, source_target_pairs={{0,4},{4,8},{8,12},{12,16},{16,20},{20,24},{24,28},{1,5},{5,9},{9,... | collective-permute-start | bytes 73736 | tf_op jit(solution)/shard_map/ppermute | solution.py:21
  120.7 37.0 %copy-start.5 = (bf16[512,256]{1,0:T(8,128)(2,1)S(1)}, bf16[512,256]{1,0:T(8,128)(2,1)}, u32[]{:S(2)}) copy-start(bf16[512,256]{1,0:T(8,128)(2,1)} %get-tuple-element.9) | copy-start | bytes 786436
  (2 other events, 9.4 us)
Sparse Core Ops, SparseCore 0:
  18.6 12.2 all-gather.2
  162.6 11.2 reduce-scatter.1

commit v2 on v1

--- a/solution.py
+++ b/solution.py
@@ -39,33 +39,37 @@
     return jnp.where(index % 2 == 0, index // 2, count - 1 - index // 2)
 
 
-def ring_gather(block, axis):
+def ring_blocks(block, axis):
     count, index = (lax.axis_size(axis), lax.axis_index(axis))
     half = count // 2
     order = [2 * p if p < half else 2 * (count - 1 - p) + 1 for p in range(count)]
     place = ring_place(index, count)
     onward = [(order[p], order[(p + 1) % count]) for p in range(count)]
     backward = [(order[p], order[(p - 1) % count]) for p in range(count)]
+    middle = block.shape[0] // 2
+    arrived = [(block, place, 0)]
+    right = left = block
+    for step in range(1, half + 1):
+        last = step == half
+        right = lax.ppermute(right[:middle] if last else right, axis, onward)
+        left = lax.ppermute(left[middle:] if last else left, axis, backward)
+        arrived.append((right, place - step + count, 0))
+        arrived.append((left, place + step, middle if last else 0))
     rows = block.shape[0]
-    full = jnp.zeros((rows * count, block.shape[1]), block.dtype)
-
-    def put(full, part, source, offset):
-        return lax.dynamic_update_slice(
-            full, part, (ring_order(source % count, count) * rows + offset, 0)
-        )
-
-    full = put(full, block, place, 0)
-    right = left = block
-    for step in range(1, half):
-        right = lax.ppermute(right, axis, onward)
-        left = lax.ppermute(left, axis, backward)
-        full = put(full, right, place - step + count, 0)
-        full = put(full, left, place + step, 0)
-    middle = rows // 2
-    right = lax.ppermute(right[:middle], axis, onward)
-    left = lax.ppermute(left[middle:], axis, backward)
-    full = put(full, right, place - half + count, 0)
-    return put(full, left, place + half, middle)
+    return [
+        (part, ring_order(source % count, count) * rows + offset)
+        for part, source, offset in arrived
+    ]
+
+
+def lane_aligned(blocks):
+    if all(part.shape[0] % 128 == 0 for part, _ in blocks):
+        return blocks
+    rows = lax.axis_size("sp") * blocks[0][0].shape[0]
+    full = jnp.zeros((rows, blocks[0][0].shape[1]), blocks[0][0].dtype)
+    for part, start in blocks:
+        full = lax.dynamic_update_slice(full, part, (start, 0))
+    return [(full, jnp.zeros((), jnp.int32))]
 
 
 def one_minus_exp(x):
@@ -154,23 +158,44 @@
         end_ref[1:2, cols] = end_state
 
 
-def finish_kernel(where_ref, gate_ref, cum_ref, state_ref, ends_ref, initial_ref, out_ref):
+def exit_columns(out_ref, starts_ref, pool_rows, rnn_rows, blocks):
+    pool_width = pool_rows.shape[1]
+    contract = (((1,), (1,)), ((), ()))
+    for k, block in enumerate(blocks):
+        size = block.shape[0]
+        at = pl.ds(pl.multiple_of(starts_ref[k], 128), size)
+        total = lax.dot_general(
+            pool_rows, block[:, :pool_width], contract, preferred_element_type=jnp.float32
+        ) + lax.dot_general(
+            rnn_rows, block[:, pool_width:], contract, preferred_element_type=jnp.float32
+        )
+        out_ref[:, at] = total.astype(out_ref.dtype)
+
+
+def finish_kernel(where_ref, starts_ref, gate_ref, cum_ref, state_ref, carried_ref, pool_ref, *refs):
+    blocks, (rnn_ref, away_ref) = refs[:-2], refs[-2:]
     rows = gate_ref.shape[0]
     width = 2 * HEAD_DIM
-    carried = initial_ref[...]
-    for k in range(ends_ref.shape[0] // 2):
-        after = carried * ends_ref[2 * k : 2 * k + 1] + ends_ref[2 * k + 1 : 2 * k + 2]
-        carried = jnp.where(k < where_ref[1], after, carried)
     length = rows // SEGMENTS
     for p in range(cum_ref.shape[0]):
         cols = slice(p * width, (p + 1) * width)
-        before = carried[:, cols]
+        before = carried_ref[:, cols]
         for s in range(SEGMENTS):
             span = slice(s * length, (s + 1) * length)
             hidden = state_ref[p, span] + cum_ref[p, span] * before
             gate = jax.nn.gelu(gate_ref[span, cols].astype(jnp.float32), approximate=True)
-            out_ref[span, cols] = (gate * hidden).astype(jnp.bfloat16)
+            rnn_ref[span, cols] = (gate * hidden).astype(jnp.bfloat16)
             before = hidden[length - 1 : length]
+    half = rows // 2
+    span = pl.ds(pl.multiple_of((1 - where_ref[0]) * half, 128), half)
+    exit_columns(away_ref, starts_ref, pool_ref[span, :], rnn_ref[span, :], blocks)
+
+
+def keep_kernel(where_ref, starts_ref, pool_ref, rnn_ref, *refs):
+    blocks, out_ref = refs[:-1], refs[-1]
+    half = pool_ref.shape[0] // 2
+    span = pl.ds(pl.multiple_of(where_ref[0] * half, 128), half)
+    exit_columns(out_ref, starts_ref, pool_ref[span, :], rnn_ref[span, :], blocks)
 
 
 def shards(
@@ -193,14 +218,31 @@
     tp_index = lax.axis_index("tp")
     sp_index = lax.axis_index("sp")
     where = jnp.stack([tp_index, sp_index]).astype(jnp.int32)
-    weight_in = ring_gather(jnp.concatenate([pool_in, value_in, gate_in], axis=1), "sp")
-    weight_out = ring_gather(jnp.concatenate([out_pool, out_rnn], axis=1), "sp")
+    swap = [(t, t ^ 1) for t in range(lax.axis_size("tp"))]
+    blocks_in = ring_blocks(jnp.concatenate([pool_in, value_in, gate_in], axis=1), "sp")
+    own_out = jnp.concatenate([out_pool, out_rnn], axis=1)
+    own_out, last_right, last_left = lax.optimization_barrier(
+        (own_out, blocks_in[-2][0], blocks_in[-1][0])
+    )
+    blocks_in[-2] = (last_right, blocks_in[-2][1])
+    blocks_in[-1] = (last_left, blocks_in[-1][1])
+    blocks_out = lane_aligned(ring_blocks(own_out, "sp"))
     pool_width = pool_in.shape[1]
     rnn_width = gate_in.shape[1]
-    widened = lax.all_gather(tokens, "tp", axis=0, tiled=True).astype(jnp.float32)
+    widened = tokens.astype(jnp.float32)
     scaling = lax.rsqrt(jnp.mean(widened * widened, axis=1, keepdims=True) + epsilon)
-    normed = (widened * scaling * norm_gain[None, :]).astype(jnp.bfloat16)
-    projected = jnp.dot(normed, weight_in, preferred_element_type=jnp.float32).astype(jnp.bfloat16)
+    normed_own = (widened * scaling * norm_gain[None, :]).astype(jnp.bfloat16)
+    normed_peer = lax.ppermute(normed_own, "tp", swap)
+    first = tp_index == 0
+    normed = jnp.concatenate(
+        [jnp.where(first, normed_own, normed_peer), jnp.where(first, normed_peer, normed_own)],
+        axis=0,
+    )
+    summed = jnp.zeros((normed.shape[0], pool_width + 2 * rnn_width), jnp.float32)
+    for part, start in blocks_in:
+        columns = lax.dynamic_slice_in_dim(normed, start, part.shape[0], axis=1)
+        summed = summed + jnp.dot(columns, part, preferred_element_type=jnp.float32)
+    projected = summed.astype(jnp.bfloat16)
     block_rows = projected.shape[0]
     front_width = pool_width + rnn_width
     pool_pre = projected[:, :pool_width]
@@ -244,16 +286,43 @@
         rate,
         jnp.transpose(decay_shift),
     )
-    all_ends = lax.all_gather(ends, "sp", axis=0, tiled=True)
-    rnn_out = pl.pallas_call(
+    count = lax.axis_size("sp")
+    through = ends
+    reach = 1
+    while reach < count:
+        earlier = from_behind(through, "sp", reach)
+        product = earlier[:1] * through[:1]
+        state = through[:1] * earlier[1:] + through[1:]
+        through = jnp.where(
+            sp_index >= reach, jnp.concatenate([product, state], axis=0), through
+        )
+        reach *= 2
+    initial = initial_state[None, :]
+    reached = through[:1] * initial + through[1:]
+    carried = jnp.where(sp_index == 0, initial, from_behind(reached, "sp", 1))
+    out_parts = [part for part, _ in blocks_out]
+    starts = jnp.stack([start for _, start in blocks_out]).astype(jnp.int32)
+    half_rows = block_rows // 2
+    features = own_out.shape[0] * count
+    rnn_out, away = pl.pallas_call(
         finish_kernel,
-        out_shape=jax.ShapeDtypeStruct((block_rows, rnn_width), jnp.bfloat16),
-        in_specs=[smem] + [vmem] * 5,
+        out_shape=(
+            jax.ShapeDtypeStruct((block_rows, rnn_width), jnp.bfloat16),
+            jax.ShapeDtypeStruct((half_rows, features), jnp.bfloat16),
+        ),
+        in_specs=[smem, smem] + [vmem] * (5 + len(out_parts)),
+        out_specs=(vmem, vmem),
+        name="finish",
+    )(where, starts, gate_pre, cumulative, local_state, carried, pool_out, *out_parts)
+    arriving = lax.ppermute(away, "tp", swap)
+    kept = pl.pallas_call(
+        keep_kernel,
+        out_shape=jax.ShapeDtypeStruct((half_rows, features), jnp.float32),
+        in_specs=[smem, smem] + [vmem] * (2 + len(out_parts)),
         out_specs=vmem,
-        name="finish",
-    )(where, gate_pre, cumulative, local_state, all_ends, initial_state[None, :])
-    partial = right_product(jnp.concatenate([pool_out, rnn_out], axis=1), weight_out)
-    return lax.psum_scatter(partial, "tp", scatter_dimension=0, tiled=True).astype(jnp.bfloat16)
+        name="keep",
+    )(where, starts, pool_out, rnn_out, *out_parts)
+    return (kept + arriving.astype(jnp.float32)).astype(jnp.bfloat16)
 
 
 def solution(mesh):

time: 184 us -> 139 us (0.76)
  blocking collectives: 33.3 us -> 0 us
  local copies, waits for them, and re-layouts: 30.2 us -> 7.37 us
  starting transfers between devices: 20.2 us -> 35.8 us
  between operations: 13.6 us -> 0.34 us
  Pallas kernels: 11.2 us -> 18 us
  other arithmetic: 6.91 us -> 13.3 us
  waiting for transfers between devices: 57.8 us -> 55.5 us
  matrix products: 10.2 us -> 8.1 us
    all_gather x1 -> x0, blocking collectives: 33.3 us -> none  [shards(): all_ends = lax.all_gather(ends, 'sp', axis=0, tiled=True)]
    dynamic_update_slice x18 -> x0, local copies, waits for them, and re-layouts: 15.2 us -> none  [put(): lax.dynamic_update_slice(full, part, (ring_order(source % count, count) *...]
    ppermute x1 -> x5, starting transfers between devices: 2.62 us -> 16.8 us  [from_behind(): lax.ppermute(value, axis, [(source, source + steps) for source in range(f...]
    reduce_scatter x1 -> x0, waiting for transfers between devices: 11.4 us -> none  [shards(): lax.psum_scatter(partial, 'tp', scatter_dimension=0, tiled=True)]
    pallas_call x1 -> x2, Pallas kernels: 3.02 us -> 9.83 us  [the longest x1 5.29 us: shards(): pl.pallas_call(finish_kernel, out_shape=(jax.ShapeDtypeStruct((block_rows...]
    ppermute x1 -> x5, waiting for transfers between devices: 0.01 us -> 5.49 us  [from_behind(): lax.ppermute(value, axis, [(source, source + steps) for source in range(f...]
    ppermute x16 -> x18, waiting for transfers between devices: 46.3 us -> 50 us  [the longest x8 35.8 us: ring_blocks(): right = lax.ppermute(right[:middle] if last else right, axis, onward)]
    select_n x0 -> x5, other arithmetic: none -> 3.41 us  [the longest x3 2.1 us: shards(): jnp.where(sp_index >= reach, jnp.concatenate([product, state], axis=0), t...]
  transfers between devices with their start and end apart: 19 -> 23, of which waited for: 9 -> 12; matrix products, arithmetic and copies ran while one was open for 14% -> 14% of each run, Pallas kernels for 0% -> 3%
where the time goes in v2:
time: 139 us; the launch traced here: 138 us
  waiting for transfers between devices  55.5 us (40%)
  starting transfers between devices  35.8 us (26%)
  Pallas kernels  18 us (13%)
  other arithmetic  13.3 us (10%)
  matrix products  8.1 us (6%)
  local copies, waits for them, and re-layouts  7.37 us (5%)
    ppermute x8, waiting for transfers between devices, ring_blocks(): right = lax.ppermute(right[:middle] if last else right, axis, onward)  35.8 us
    ppermute x5, starting transfers between devices, from_behind(): lax.ppermute(value, axis, [(source, source + steps) for source in range(f...  16.8 us
    ppermute x8, waiting for transfers between devices, ring_blocks(): left = lax.ppermute(left[middle:] if last else left, axis, backward)  14.2 us
    ppermute x8, starting transfers between devices, ring_blocks(): left = lax.ppermute(left[middle:] if last else left, axis, backward)  13 us
    pallas_call x1, Pallas kernels, shards(): pl.pallas_call(mixer_kernel, out_shape=(jax.ShapeDtypeStruct((block_rows,...  8.19 us
    dot_general x9, matrix products, shards(): summed = summed + jnp.dot(columns, part, preferred_element_type=jnp.float32)  8.1 us
    ppermute x8, starting transfers between devices, ring_blocks(): right = lax.ppermute(right[:middle] if last else right, axis, onward)  5.52 us
    ppermute x5, waiting for transfers between devices, from_behind(): lax.ppermute(value, axis, [(source, source + steps) for source in range(f...  5.49 us
  transfers between devices with their start and end apart: 23, of which 12 were waited for; matrix products, arithmetic and copies ran while one was open for 14% of the time, Pallas kernels for 3%

profile of v2, /device:TPU:0, one launch (start us, length us, event | category | flops | bytes accessed | tf_op | source)
XLA Modules:
  0.0 138.5 jit_solution(17189150717343716094)
XLA Ops:
  5.9 2.5 %collective-permute-start.2 = (bf16[256,1280]{1,0:T(8,128)(2,1)}, bf16[256,1280]{1,0:T(8,128)(2,1)}, u32[]{:S(2)}, u32[]{:S(2)}) collective-permute-start(bf16[256,1280]{1,0:T(8,128)(2,1)} %constant_dynamic-update-slice_fusion), channel_id=1, source_target_pairs={{0,4},{8,0},{16,8},{24,16},{28,24},{20,28},{12,20},{4,12},{1,5},{9... | collective-permute-start | bytes 1966088 | tf_op jit(solution)/shard_map/ppermute | solution.py:55
  12.5 11.7 %collective-permute-done.2 = bf16[256,1280]{1,0:T(8,128)(2,1)} collective-permute-done((bf16[256,1280]{1,0:T(8,128)(2,1)}, bf16[256,1280]{1,0:T(8,128)(2,1)}, u32[]{:S(2)}, u32[]{:S(2)}) %collective-permute-start.2) | collective-permute-done | bytes 655392 | tf_op jit(solution)/shard_map/ppermute | solution.py:55
  24.2 1.7 %collective-permute-start.4 = (bf16[256,1280]{1,0:T(8,128)(2,1)}, bf16[256,1280]{1,0:T(8,128)(2,1)S(1)}, u32[]{:S(2)}, u32[]{:S(2)}) collective-permute-start(bf16[256,1280]{1,0:T(8,128)(2,1)} %collective-permute-done.2), channel_id=1, source_target_pairs={{0,4},{8,0},{16,8},{24,16},{28,24},{20,28},{12,20},{4,12},{1,5},{9... | collective-permute-start | bytes 1966088 | tf_op jit(solution)/shard_map/ppermute | solution.py:55
  27.0 1.6 %fusion.31 = f32[512,1280]{1,0:T(8,128)S(1)} fusion(bf16[256,1280]{1,0:T(8,128)(2,1)} %collective-permute-done.2, s32[]{:T(128)S(6)} %select_n.201, bf16[256,2048]{1,0:T(8,128)(2,1)S(1)} %get-tuple-element.24, bf16[256,2048]{1,0:T(8,128)(2,1)S(1)} %get-tuple-element.23), kind=kOutput, calls=%fused_computation.60 | convolution fusion | flops 336068608 | bytes 5373956 | tf_op jit(solution)/shard_map/dot_general | solution.py:244
  30.2 11.9 %collective-permute-done.3 = bf16[256,1280]{1,0:T(8,128)(2,1)S(1)} collective-permute-done((bf16[256,1280]{1,0:T(8,128)(2,1)}, bf16[256,1280]{1,0:T(8,128)(2,1)S(1)}, u32[]{:S(2)}, u32[]{:S(2)}) %collective-permute-start.3) | collective-permute-done | bytes 655392 | tf_op jit(solution)/shard_map/ppermute | solution.py:54
  44.1 1.6 %fusion.2 = f32[512,1280]{1,0:T(8,128)S(1)} fusion(f32[512,1280]{1,0:T(8,128)S(1)} %fusion.31, f32[512,1280]{1,0:T(8,128)S(1)} %fusion.29, bf16[256,1280]{1,0:T(8,128)(2,1)} %constant_dynamic-update-slice_fusion, s32[]{:T(128)S(6)} %select_n.199, bf16[256,2048]{1,0:T(8,128)(2,1)S(1)} %get-tuple-element.24, bf16[256,2048]{1,0:T(8,128)(2,1)S(1)} %get-tuple-element.23), kind=kOutput, calls=%fused_computation.23 | convolution fusion | flops 337379328 | bytes 10616836 | tf_op jit(solution)/shard_map/dot_general | solution.py:244
  46.3 11.0 %collective-permute-done.5 = bf16[256,1280]{1,0:T(8,128)(2,1)S(1)} collective-permute-done((bf16[256,1280]{1,0:T(8,128)(2,1)S(1)}, bf16[256,1280]{1,0:T(8,128)(2,1)S(1)}, u32[]{:S(2)}, u32[]{:S(2)}) %collective-permute-start.5) | collective-permute-done | bytes 655392 | tf_op jit(solution)/shard_map/ppermute | solution.py:54
  60.6 4.0 %collective-permute-done.7 = bf16[128,1280]{1,0:T(8,128)(2,1)S(1)} collective-permute-done((bf16[128,1280]{1,0:T(8,128)(2,1)S(1)}, bf16[128,1280]{1,0:T(8,128)(2,1)S(1)}, u32[]{:S(2)}, u32[]{:S(2)}) %collective-permute-start.7) | collective-permute-done | bytes 327712 | tf_op jit(solution)/shard_map/ppermute | solution.py:54
  67.3 2.9 %collective-permute-start.9 = (bf16[16,768]{1,0:T(8,128)(2,1)S(1)}, bf16[16,768]{1,0:T(8,128)(2,1)S(1)}, u32[]{:S(2)}, u32[]{:S(2)}) collective-permute-start(bf16[16,768]{1,0:T(8,128)(2,1)S(1)} %slice.119), channel_id=1, source_target_pairs={{0,4},{4,8},{8,12},{12,16},{16,20},{20,24},{24,28},{1,5},{5,9},{9,... | collective-permute-start | bytes 73736 | tf_op jit(solution)/shard_map/ppermute | solution.py:21
  73.1 8.2 %mixer.1 = (bf16[512,256]{1,0:T(8,128)(2,1)}, f32[4,512,128]{2,1,0:T(8,128)}, f32[4,512,128]{2,1,0:T(8,128)}, f32[2,512]{1,0:T(2,128)}) custom-call(s32[2]{0:T(128)} %pad_add_fusion.where_ref, bf16[512,256]{1,0:T(8,128)(2,1)} %slice.117.pool_ref, bf16[512,512]{1,0:T(8,128)(2,1)} %get-tuple-element.26.value_ref, bf16[16,256]{1,0:T(8,128)(2,1)} %slice.120.edge_pool_ref, ...), custom_call_target="tpu_custom_call" | custom-call | tf_op jit(solution)/shard_map/mixer/pallas_call | solution.py:265
  81.3 3.9 %collective-permute-start.10 = (f32[2,512]{1,0:T(2,128)}, f32[2,512]{1,0:T(2,128)S(1)}, u32[]{:S(2)}, u32[]{:S(2)}) collective-permute-start(f32[2,512]{1,0:T(2,128)} %get-tuple-element.19), channel_id=1, source_target_pairs={{0,4},{4,8},{8,12},{12,16},{16,20},{20,24},{24,28},{1,5},{5,9},{9,... | collective-permute-start | bytes 12296 | tf_op jit(solution)/shard_map/ppermute | solution.py:21
  85.2 1.6 %collective-permute-start.14 = (bf16[256,768]{1,0:T(8,128)(2,1)S(1)}, bf16[256,768]{1,0:T(8,128)(2,1)S(1)}, u32[]{:S(2)}, u32[]{:S(2)}) collective-permute-start(bf16[256,768]{1,0:T(8,128)(2,1)S(1)} %pad_maximum_fusion.refs_0_), channel_id=1, source_target_pairs={{0,8},{8,16},{16,24},{24,28},{28,20},{20,12},{12,4},{4,0},{1,9},{9... | collective-permute-start | bytes 1179656 | tf_op jit(solution)/shard_map/ppermute | solution.py:54
  89.2 4.3 %collective-permute-start.11 = (f32[2,512]{1,0:T(2,128)S(1)}, f32[2,512]{1,0:T(2,128)S(1)}, u32[]{:S(2)}, u32[]{:S(2)}) collective-permute-start(f32[2,512]{1,0:T(2,128)S(1)} %maximum_select_fusion), channel_id=1, source_target_pairs={{0,8},{4,12},{8,16},{12,20},{16,24},{20,28},{1,9},{5,13},{9,17},{1... | collective-permute-start | bytes 12296 | tf_op jit(solution)/shard_map/ppermute | solution.py:21
  99.6 2.6 %collective-permute-start.12 = (f32[2,512]{1,0:T(2,128)S(1)}, f32[2,512]{1,0:T(2,128)S(1)}, u32[]{:S(2)}, u32[]{:S(2)}) collective-permute-start(f32[2,512]{1,0:T(2,128)S(1)} %maximum_select_fusion.1), channel_id=1, source_target_pairs={{0,16},{4,20},{8,24},{12,28},{1,17},{5,21},{9,25},{13,29},{2,18},{... | collective-permute-start | bytes 12296 | tf_op jit(solution)/shard_map/ppermute | solution.py:21
  102.3 4.2 %collective-permute-done.12 = f32[2,512]{1,0:T(2,128)S(1)} collective-permute-done((f32[2,512]{1,0:T(2,128)S(1)}, f32[2,512]{1,0:T(2,128)S(1)}, u32[]{:S(2)}, u32[]{:S(2)}) %collective-permute-start.12) | collective-permute-done | bytes 4128 | tf_op jit(solution)/shard_map/ppermute | solution.py:21
  106.4 2.3 %collective-permute-done.16.refs_3_ = bf16[256,768]{1,0:T(8,128)(2,1)S(1)} collective-permute-done((bf16[256,768]{1,0:T(8,128)(2,1)S(1)}, bf16[256,768]{1,0:T(8,128)(2,1)S(1)}, u32[]{:S(2)}, u32[]{:S(2)}) %collective-permute-start.16) | collective-permute-done | bytes 393248 | tf_op jit(solution)/shard_map/ppermute | solution.py:54
  108.9 1.9 %collective-permute-start.19 = (bf16[256,768]{1,0:T(8,128)(2,1)S(1)}, bf16[256,768]{1,0:T(8,128)(2,1)S(1)}, u32[]{:S(2)}, u32[]{:S(2)}) collective-permute-start(bf16[256,768]{1,0:T(8,128)(2,1)S(1)} %collective-permute-done.17.refs_4_), channel_id=1, source_target_pairs={{0,4},{8,0},{16,8},{24,16},{28,24},{20,28},{12,20},{4,12},{1,5},{9... | collective-permute-start | bytes 1179656 | tf_op jit(solution)/shard_map/ppermute | solution.py:55
  111.5 3.0 %collective-permute-start.13 = (f32[1,512]{1,0:T(1,128)S(1)}, f32[1,512]{1,0:T(1,128)S(1)}, u32[]{:S(2)}, u32[]{:S(2)}) collective-permute-start(f32[1,512]{1,0:T(1,128)S(1)} %slice_add_fusion), channel_id=1, source_target_pairs={{0,4},{4,8},{8,12},{12,16},{16,20},{20,24},{24,28},{1,5},{5,9},{9,... | collective-permute-start | bytes 6152 | tf_op jit(solution)/shard_map/ppermute | solution.py:21
  115.2 2.7 %collective-permute-done.18.refs_5_ = bf16[256,768]{1,0:T(8,128)(2,1)S(1)} collective-permute-done((bf16[256,768]{1,0:T(8,128)(2,1)S(1)}, bf16[256,768]{1,0:T(8,128)(2,1)S(1)}, u32[]{:S(2)}, u32[]{:S(2)}) %collective-permute-start.18) | collective-permute-done | bytes 393248 | tf_op jit(solution)/shard_map/ppermute | solution.py:54
  118.5 1.7 %collective-permute-start.21 = (bf16[128,768]{1,0:T(8,128)(2,1)S(1)}, bf16[128,768]{1,0:T(8,128)(2,1)S(1)}, u32[]{:S(2)}, u32[]{:S(2)}) collective-permute-start(bf16[128,768]{1,0:T(8,128)(2,1)S(1)} %slice.140), channel_id=1, source_target_pairs={{0,4},{8,0},{16,8},{24,16},{28,24},{20,28},{12,20},{4,12},{1,5},{9... | collective-permute-start | bytes 589832 | tf_op jit(solution)/shard_map/ppermute | solution.py:55
  120.8 2.8 %collective-permute-done.20.refs_7_ = bf16[128,768]{1,0:T(8,128)(2,1)S(1)} collective-permute-done((bf16[128,768]{1,0:T(8,128)(2,1)S(1)}, bf16[128,768]{1,0:T(8,128)(2,1)S(1)}, u32[]{:S(2)}, u32[]{:S(2)}) %collective-permute-start.20) | collective-permute-done | bytes 196640 | tf_op jit(solution)/shard_map/ppermute | solution.py:54
  125.8 5.3 %finish.1 = (bf16[512,512]{1,0:T(8,128)(2,1)}, bf16[256,2048]{1,0:T(8,128)(2,1)}) custom-call(s32[2]{0:T(128)} %pad_add_fusion.where_ref, s32[9]{0:T(128)} %stack.51.starts_ref, bf16[512,512]{1,0:T(8,128)(2,1)} %get-tuple-element.25.gate_ref, f32[4,512,128]{2,1,0:T(8,128)} %get-tuple-element.17.cum_ref, f32[4,512,128]{2,1,0:T(8,128)} %get-tuple-element.18.state_ref, ...), custom_call_target="tpu_custom_call" | custom-call | tf_op jit(solution)/shard_map/finish/pallas_call | solution.py:307
  131.1 4.5 %keep.1 = f32[256,2048]{1,0:T(8,128)} custom-call(s32[2]{0:T(128)} %pad_add_fusion.where_ref, s32[9]{0:T(128)} %stack.51.starts_ref, bf16[512,256]{1,0:T(8,128)(2,1)} %get-tuple-element.16.pool_ref, bf16[512,512]{1,0:T(8,128)(2,1)} %get-tuple-element.21.rnn_ref, bf16[256,768]{1,0:T(8,128)(2,1)} %copy-done.1, bf16[256,768]{1,0:T(8,128)(2,1)} %copy-done.4, ...), custom_call_target="tpu_custom_call" | custom-call | tf_op jit(solution)/shard_map/keep/pallas_call | solution.py:318
  135.6 2.8 %add_convert_fusion = bf16[256,2048]{1,0:T(8,128)(2,1)} fusion(f32[256,2048]{1,0:T(8,128)} %keep.1, bf16[256,2048]{1,0:T(8,128)(2,1)S(1)} %collective-permute-done.22), kind=kLoop, calls=%fused_computation.32 | loop fusion | flops 1572864 | bytes 4194304 | tf_op jit(solution)/shard_map/convert_element_type | solution.py:325
  (104 shorter events, 37.2 us)
Async XLA Ops:
  3.3 23.0 %collective-permute-start = (bf16[256,2048]{1,0:T(8,128)(2,1)S(1)}, bf16[256,2048]{1,0:T(8,128)(2,1)S(1)}, u32[]{:S(2)}, u32[]{:S(2)}) collective-permute-start(bf16[256,2048]{1,0:T(8,128)(2,1)S(1)} %fusion.8), channel_id=1, source_target_pairs={{0,1},{1,0},{2,3},{3,2},{4,5},{5,4},{6,7},{7,6},{8,9},{9,8},{10,11... | collective-permute-start | bytes 3145736 | tf_op jit(solution)/shard_map/ppermute | solution.py:235
  5.9 18.3 %collective-permute-start.2 = (bf16[256,1280]{1,0:T(8,128)(2,1)}, bf16[256,1280]{1,0:T(8,128)(2,1)}, u32[]{:S(2)}, u32[]{:S(2)}) collective-permute-start(bf16[256,1280]{1,0:T(8,128)(2,1)} %constant_dynamic-update-slice_fusion), channel_id=1, source_target_pairs={{0,4},{8,0},{16,8},{24,16},{28,24},{20,28},{12,20},{4,12},{1,5},{9... | collective-permute-start | bytes 1966088 | tf_op jit(solution)/shard_map/ppermute | solution.py:55
  8.5 17.4 %collective-permute-start.1 = (bf16[256,1280]{1,0:T(8,128)(2,1)}, bf16[256,1280]{1,0:T(8,128)(2,1)}, u32[]{:S(2)}, u32[]{:S(2)}) collective-permute-start(bf16[256,1280]{1,0:T(8,128)(2,1)} %constant_dynamic-update-slice_fusion), channel_id=1, source_target_pairs={{0,8},{8,16},{16,24},{24,28},{28,20},{20,12},{12,4},{4,0},{1,9},{9... | collective-permute-start | bytes 1966088 | tf_op jit(solution)/shard_map/ppermute | solution.py:54
  11.9 75.0 %copy-start.1 = (bf16[256,768]{1,0:T(8,128)(2,1)}, bf16[256,768]{1,0:T(8,128)(2,1)S(1)}, u32[]{:S(2)}) copy-start(bf16[256,768]{1,0:T(8,128)(2,1)S(1)} %pad_maximum_fusion.refs_0_) | copy-start | bytes 1179652
  24.2 18.5 %collective-permute-start.4 = (bf16[256,1280]{1,0:T(8,128)(2,1)}, bf16[256,1280]{1,0:T(8,128)(2,1)S(1)}, u32[]{:S(2)}, u32[]{:S(2)}) collective-permute-start(bf16[256,1280]{1,0:T(8,128)(2,1)} %collective-permute-done.2), channel_id=1, source_target_pairs={{0,4},{8,0},{16,8},{24,16},{28,24},{20,28},{12,20},{4,12},{1,5},{9... | collective-permute-start | bytes 1966088 | tf_op jit(solution)/shard_map/ppermute | solution.py:55
  25.9 16.2 %collective-permute-start.3 = (bf16[256,1280]{1,0:T(8,128)(2,1)}, bf16[256,1280]{1,0:T(8,128)(2,1)S(1)}, u32[]{:S(2)}, u32[]{:S(2)}) collective-permute-start(bf16[256,1280]{1,0:T(8,128)(2,1)} %collective-permute-done.1), channel_id=1, source_target_pairs={{0,8},{8,16},{16,24},{24,28},{28,20},{20,12},{12,4},{4,0},{1,9},{9... | collective-permute-start | bytes 1966088 | tf_op jit(solution)/shard_map/ppermute | solution.py:54
  42.1 15.1 %collective-permute-start.5 = (bf16[256,1280]{1,0:T(8,128)(2,1)S(1)}, bf16[256,1280]{1,0:T(8,128)(2,1)S(1)}, u32[]{:S(2)}, u32[]{:S(2)}) collective-permute-start(bf16[256,1280]{1,0:T(8,128)(2,1)S(1)} %collective-permute-done.3), channel_id=1, source_target_pairs={{0,8},{8,16},{16,24},{24,28},{28,20},{20,12},{12,4},{4,0},{1,9},{9... | collective-permute-start | bytes 1966088 | tf_op jit(solution)/shard_map/ppermute | solution.py:54
  42.7 15.5 %collective-permute-start.6 = (bf16[256,1280]{1,0:T(8,128)(2,1)S(1)}, bf16[256,1280]{1,0:T(8,128)(2,1)S(1)}, u32[]{:S(2)}, u32[]{:S(2)}) collective-permute-start(bf16[256,1280]{1,0:T(8,128)(2,1)S(1)} %collective-permute-done.4), channel_id=1, source_target_pairs={{0,4},{8,0},{16,8},{24,16},{28,24},{20,28},{12,20},{4,12},{1,5},{9... | collective-permute-start | bytes 1966088 | tf_op jit(solution)/shard_map/ppermute | solution.py:55
  57.3 7.3 %collective-permute-start.7 = (bf16[128,1280]{1,0:T(8,128)(2,1)S(1)}, bf16[128,1280]{1,0:T(8,128)(2,1)S(1)}, u32[]{:S(2)}, u32[]{:S(2)}) collective-permute-start(bf16[128,1280]{1,0:T(8,128)(2,1)S(1)} %slice.115), channel_id=1, source_target_pairs={{0,8},{8,16},{16,24},{24,28},{28,20},{20,12},{12,4},{4,0},{1,9},{9... | collective-permute-start | bytes 983048 | tf_op jit(solution)/shard_map/ppermute | solution.py:54
  58.3 7.3 %collective-permute-start.8 = (bf16[128,1280]{1,0:T(8,128)(2,1)S(1)}, bf16[128,1280]{1,0:T(8,128)(2,1)S(1)}, u32[]{:S(2)}, u32[]{:S(2)}) collective-permute-start(bf16[128,1280]{1,0:T(8,128)(2,1)S(1)} %slice.116), channel_id=1, source_target_pairs={{0,4},{8,0},{16,8},{24,16},{28,24},{20,28},{12,20},{4,12},{1,5},{9... | collective-permute-start | bytes 983048 | tf_op jit(solution)/shard_map/ppermute | solution.py:55
  67.3 4.7 %collective-permute-start.9 = (bf16[16,768]{1,0:T(8,128)(2,1)S(1)}, bf16[16,768]{1,0:T(8,128)(2,1)S(1)}, u32[]{:S(2)}, u32[]{:S(2)}) collective-permute-start(bf16[16,768]{1,0:T(8,128)(2,1)S(1)} %slice.119), channel_id=1, source_target_pairs={{0,4},{4,8},{8,12},{12,16},{16,20},{20,24},{24,28},{1,5},{5,9},{9,... | collective-permute-start | bytes 73736 | tf_op jit(solution)/shard_map/ppermute | solution.py:21
  81.3 6.5 %collective-permute-start.10 = (f32[2,512]{1,0:T(2,128)}, f32[2,512]{1,0:T(2,128)S(1)}, u32[]{:S(2)}, u32[]{:S(2)}) collective-permute-start(f32[2,512]{1,0:T(2,128)} %get-tuple-element.19), channel_id=1, source_target_pairs={{0,4},{4,8},{8,12},{12,16},{16,20},{20,24},{24,28},{1,5},{5,9},{9,... | collective-permute-start | bytes 12296 | tf_op jit(solution)/shard_map/ppermute | solution.py:21
  85.2 10.8 %collective-permute-start.14 = (bf16[256,768]{1,0:T(8,128)(2,1)S(1)}, bf16[256,768]{1,0:T(8,128)(2,1)S(1)}, u32[]{:S(2)}, u32[]{:S(2)}) collective-permute-start(bf16[256,768]{1,0:T(8,128)(2,1)S(1)} %pad_maximum_fusion.refs_0_), channel_id=1, source_target_pairs={{0,8},{8,16},{16,24},{24,28},{28,20},{20,12},{12,4},{4,0},{1,9},{9... | collective-permute-start | bytes 1179656 | tf_op jit(solution)/shard_map/ppermute | solution.py:54
  86.9 10.4 %collective-permute-start.15 = (bf16[256,768]{1,0:T(8,128)(2,1)S(1)}, bf16[256,768]{1,0:T(8,128)(2,1)S(1)}, u32[]{:S(2)}, u32[]{:S(2)}) collective-permute-start(bf16[256,768]{1,0:T(8,128)(2,1)S(1)} %pad_maximum_fusion.refs_0_), channel_id=1, source_target_pairs={{0,4},{8,0},{16,8},{24,16},{28,24},{20,28},{12,20},{4,12},{1,5},{9... | collective-permute-start | bytes 1179656 | tf_op jit(solution)/shard_map/ppermute | solution.py:55
  89.2 5.6 %collective-permute-start.11 = (f32[2,512]{1,0:T(2,128)S(1)}, f32[2,512]{1,0:T(2,128)S(1)}, u32[]{:S(2)}, u32[]{:S(2)}) collective-permute-start(f32[2,512]{1,0:T(2,128)S(1)} %maximum_select_fusion), channel_id=1, source_target_pairs={{0,8},{4,12},{8,16},{12,20},{16,24},{20,28},{1,9},{5,13},{9,17},{1... | collective-permute-start | bytes 12296 | tf_op jit(solution)/shard_map/ppermute | solution.py:21
  96.0 12.8 %collective-permute-start.16 = (bf16[256,768]{1,0:T(8,128)(2,1)S(1)}, bf16[256,768]{1,0:T(8,128)(2,1)S(1)}, u32[]{:S(2)}, u32[]{:S(2)}) collective-permute-start(bf16[256,768]{1,0:T(8,128)(2,1)S(1)} %collective-permute-done.14.refs_1_), channel_id=1, source_target_pairs={{0,8},{8,16},{16,24},{24,28},{28,20},{20,12},{12,4},{4,0},{1,9},{9... | collective-permute-start | bytes 1179656 | tf_op jit(solution)/shard_map/ppermute | solution.py:54
  97.3 11.6 %collective-permute-start.17 = (bf16[256,768]{1,0:T(8,128)(2,1)S(1)}, bf16[256,768]{1,0:T(8,128)(2,1)S(1)}, u32[]{:S(2)}, u32[]{:S(2)}) collective-permute-start(bf16[256,768]{1,0:T(8,128)(2,1)S(1)} %collective-permute-done.15.refs_2_), channel_id=1, source_target_pairs={{0,4},{8,0},{16,8},{24,16},{28,24},{20,28},{12,20},{4,12},{1,5},{9... | collective-permute-start | bytes 1179656 | tf_op jit(solution)/shard_map/ppermute | solution.py:55
  99.6 6.8 %collective-permute-start.12 = (f32[2,512]{1,0:T(2,128)S(1)}, f32[2,512]{1,0:T(2,128)S(1)}, u32[]{:S(2)}, u32[]{:S(2)}) collective-permute-start(f32[2,512]{1,0:T(2,128)S(1)} %maximum_select_fusion.1), channel_id=1, source_target_pairs={{0,16},{4,20},{8,24},{12,28},{1,17},{5,21},{9,25},{13,29},{2,18},{... | collective-permute-start | bytes 12296 | tf_op jit(solution)/shard_map/ppermute | solution.py:21
  108.8 9.1 %collective-permute-start.18 = (bf16[256,768]{1,0:T(8,128)(2,1)S(1)}, bf16[256,768]{1,0:T(8,128)(2,1)S(1)}, u32[]{:S(2)}, u32[]{:S(2)}) collective-permute-start(bf16[256,768]{1,0:T(8,128)(2,1)S(1)} %collective-permute-done.16.refs_3_), channel_id=1, source_target_pairs={{0,8},{8,16},{16,24},{24,28},{28,20},{20,12},{12,4},{4,0},{1,9},{9... | collective-permute-start | bytes 1179656 | tf_op jit(solution)/shard_map/ppermute | solution.py:54
  108.9 9.6 %collective-permute-start.19 = (bf16[256,768]{1,0:T(8,128)(2,1)S(1)}, bf16[256,768]{1,0:T(8,128)(2,1)S(1)}, u32[]{:S(2)}, u32[]{:S(2)}) collective-permute-start(bf16[256,768]{1,0:T(8,128)(2,1)S(1)} %collective-permute-done.17.refs_4_), channel_id=1, source_target_pairs={{0,4},{8,0},{16,8},{24,16},{28,24},{20,28},{12,20},{4,12},{1,5},{9... | collective-permute-start | bytes 1179656 | tf_op jit(solution)/shard_map/ppermute | solution.py:55
  111.5 8.7 %collective-permute-start.13 = (f32[1,512]{1,0:T(1,128)S(1)}, f32[1,512]{1,0:T(1,128)S(1)}, u32[]{:S(2)}, u32[]{:S(2)}) collective-permute-start(f32[1,512]{1,0:T(1,128)S(1)} %slice_add_fusion), channel_id=1, source_target_pairs={{0,4},{4,8},{8,12},{12,16},{16,20},{20,24},{24,28},{1,5},{5,9},{9,... | collective-permute-start | bytes 6152 | tf_op jit(solution)/shard_map/ppermute | solution.py:21
  117.9 5.7 %collective-permute-start.20 = (bf16[128,768]{1,0:T(8,128)(2,1)S(1)}, bf16[128,768]{1,0:T(8,128)(2,1)S(1)}, u32[]{:S(2)}, u32[]{:S(2)}) collective-permute-start(bf16[128,768]{1,0:T(8,128)(2,1)S(1)} %slice.139), channel_id=1, source_target_pairs={{0,8},{8,16},{16,24},{24,28},{28,20},{20,12},{12,4},{4,0},{1,9},{9... | collective-permute-start | bytes 589832 | tf_op jit(solution)/shard_map/ppermute | solution.py:54
  118.5 6.6 %collective-permute-start.21 = (bf16[128,768]{1,0:T(8,128)(2,1)S(1)}, bf16[128,768]{1,0:T(8,128)(2,1)S(1)}, u32[]{:S(2)}, u32[]{:S(2)}) collective-permute-start(bf16[128,768]{1,0:T(8,128)(2,1)S(1)} %slice.140), channel_id=1, source_target_pairs={{0,4},{8,0},{16,8},{24,16},{28,24},{20,28},{12,20},{4,12},{1,5},{9... | collective-permute-start | bytes 589832 | tf_op jit(solution)/shard_map/ppermute | solution.py:55
  131.1 4.6 %collective-permute-start.22 = (bf16[256,2048]{1,0:T(8,128)(2,1)}, bf16[256,2048]{1,0:T(8,128)(2,1)S(1)}, u32[]{:S(2)}, u32[]{:S(2)}) collective-permute-start(bf16[256,2048]{1,0:T(8,128)(2,1)} %get-tuple-element.22), channel_id=1, source_target_pairs={{0,1},{1,0},{2,3},{3,2},{4,5},{5,4},{6,7},{7,6},{8,9},{9,8},{10,11... | collective-permute-start | bytes 3145736 | tf_op jit(solution)/shard_map/ppermute | solution.py:317
  (18 other events, 241.9 us)

commit v3 on v2

--- a/solution.py
+++ b/solution.py
@@ -19,12 +19,6 @@
     count = lax.axis_size(axis)
     first, last = (max(0, -steps), min(count, count - steps))
     return lax.ppermute(value, axis, [(source, source + steps) for source in range(first, last)])
-
-
-def right_product(left_rows, weight_rows):
-    return lax.dot_general(
-        left_rows, weight_rows, (((1,), (1,)), ((), ())), preferred_element_type=jnp.float32
-    )
 
 
 SEGMENTS = 8
@@ -299,7 +293,8 @@
         reach *= 2
     initial = initial_state[None, :]
     reached = through[:1] * initial + through[1:]
-    carried = jnp.where(sp_index == 0, initial, from_behind(reached, "sp", 1))
+    behind = from_behind(reached, "sp", 1)
+    carried = jnp.where(sp_index == 0, initial, behind)
     out_parts = [part for part, _ in blocks_out]
     starts = jnp.stack([start for _, start in blocks_out]).astype(jnp.int32)
     half_rows = block_rows // 2
@@ -343,6 +338,7 @@
         P("sp", "tp"),
         P("sp", "tp"),
     )
+
     return jax.shard_map(
         shards, mesh=mesh, in_specs=placed, out_specs=P(("fs", "sp", "tp"), None), check_vma=False
     )

time: 139 us -> 139 us (level)
  no operation moved by 1% of the time
where the time goes in v3:
time: 139 us; the launch traced here: 138 us
  waiting for transfers between devices  55.5 us (40%)
  starting transfers between devices  35.8 us (26%)
  Pallas kernels  18 us (13%)
  other arithmetic  13.3 us (10%)
  matrix products  8.1 us (6%)
  local copies, waits for them, and re-layouts  7.37 us (5%)
    ppermute x8, waiting for transfers between devices, ring_blocks(): right = lax.ppermute(right[:middle] if last else right, axis, onward)  35.8 us
    ppermute x5, starting transfers between devices, from_behind(): lax.ppermute(value, axis, [(source, source + steps) for source in range(f...  16.8 us
    ppermute x8, waiting for transfers between devices, ring_blocks(): left = lax.ppermute(left[middle:] if last else left, axis, backward)  14.2 us
    ppermute x8, starting transfers between devices, ring_blocks(): left = lax.ppermute(left[middle:] if last else left, axis, backward)  13 us
    pallas_call x1, Pallas kernels, shards(): pl.pallas_call(mixer_kernel, out_shape=(jax.ShapeDtypeStruct((block_rows,...  8.19 us
    dot_general x9, matrix products, shards(): summed = summed + jnp.dot(columns, part, preferred_element_type=jnp.float32)  8.1 us
    ppermute x8, starting transfers between devices, ring_blocks(): right = lax.ppermute(right[:middle] if last else right, axis, onward)  5.52 us
    ppermute x5, waiting for transfers between devices, from_behind(): lax.ppermute(value, axis, [(source, source + steps) for source in range(f...  5.49 us
  transfers between devices with their start and end apart: 23, of which 12 were waited for; matrix products, arithmetic and copies ran while one was open for 14% of the time, Pallas kernels for 3%

profile of v3, /device:TPU:0, one launch (start us, length us, event | category | flops | bytes accessed | tf_op | source)
XLA Modules:
  0.0 138.5 jit_solution(17189150717343716094)
XLA Ops:
  5.9 2.5 %collective-permute-start.2 = (bf16[256,1280]{1,0:T(8,128)(2,1)}, bf16[256,1280]{1,0:T(8,128)(2,1)}, u32[]{:S(2)}, u32[]{:S(2)}) collective-permute-start(bf16[256,1280]{1,0:T(8,128)(2,1)} %constant_dynamic-update-slice_fusion), channel_id=1, source_target_pairs={{0,4},{8,0},{16,8},{24,16},{28,24},{20,28},{12,20},{4,12},{1,5},{9... | collective-permute-start | bytes 1966088 | tf_op jit(solution)/shard_map/ppermute | solution.py:49
  12.5 11.7 %collective-permute-done.2 = bf16[256,1280]{1,0:T(8,128)(2,1)} collective-permute-done((bf16[256,1280]{1,0:T(8,128)(2,1)}, bf16[256,1280]{1,0:T(8,128)(2,1)}, u32[]{:S(2)}, u32[]{:S(2)}) %collective-permute-start.2) | collective-permute-done | bytes 655392 | tf_op jit(solution)/shard_map/ppermute | solution.py:49
  24.2 1.7 %collective-permute-start.4 = (bf16[256,1280]{1,0:T(8,128)(2,1)}, bf16[256,1280]{1,0:T(8,128)(2,1)S(1)}, u32[]{:S(2)}, u32[]{:S(2)}) collective-permute-start(bf16[256,1280]{1,0:T(8,128)(2,1)} %collective-permute-done.2), channel_id=1, source_target_pairs={{0,4},{8,0},{16,8},{24,16},{28,24},{20,28},{12,20},{4,12},{1,5},{9... | collective-permute-start | bytes 1966088 | tf_op jit(solution)/shard_map/ppermute | solution.py:49
  27.0 1.6 %fusion.31 = f32[512,1280]{1,0:T(8,128)S(1)} fusion(bf16[256,1280]{1,0:T(8,128)(2,1)} %collective-permute-done.2, s32[]{:T(128)S(6)} %select_n.201, bf16[256,2048]{1,0:T(8,128)(2,1)S(1)} %get-tuple-element.24, bf16[256,2048]{1,0:T(8,128)(2,1)S(1)} %get-tuple-element.23), kind=kOutput, calls=%fused_computation.60 | convolution fusion | flops 336068608 | bytes 5373956 | tf_op jit(solution)/shard_map/dot_general | solution.py:238
  30.2 11.9 %collective-permute-done.3 = bf16[256,1280]{1,0:T(8,128)(2,1)S(1)} collective-permute-done((bf16[256,1280]{1,0:T(8,128)(2,1)}, bf16[256,1280]{1,0:T(8,128)(2,1)S(1)}, u32[]{:S(2)}, u32[]{:S(2)}) %collective-permute-start.3) | collective-permute-done | bytes 655392 | tf_op jit(solution)/shard_map/ppermute | solution.py:48
  44.1 1.6 %fusion.2 = f32[512,1280]{1,0:T(8,128)S(1)} fusion(f32[512,1280]{1,0:T(8,128)S(1)} %fusion.31, f32[512,1280]{1,0:T(8,128)S(1)} %fusion.29, bf16[256,1280]{1,0:T(8,128)(2,1)} %constant_dynamic-update-slice_fusion, s32[]{:T(128)S(6)} %select_n.199, bf16[256,2048]{1,0:T(8,128)(2,1)S(1)} %get-tuple-element.24, bf16[256,2048]{1,0:T(8,128)(2,1)S(1)} %get-tuple-element.23), kind=kOutput, calls=%fused_computation.23 | convolution fusion | flops 337379328 | bytes 10616836 | tf_op jit(solution)/shard_map/dot_general | solution.py:238
  46.3 11.0 %collective-permute-done.5 = bf16[256,1280]{1,0:T(8,128)(2,1)S(1)} collective-permute-done((bf16[256,1280]{1,0:T(8,128)(2,1)S(1)}, bf16[256,1280]{1,0:T(8,128)(2,1)S(1)}, u32[]{:S(2)}, u32[]{:S(2)}) %collective-permute-start.5) | collective-permute-done | bytes 655392 | tf_op jit(solution)/shard_map/ppermute | solution.py:48
  60.6 4.0 %collective-permute-done.7 = bf16[128,1280]{1,0:T(8,128)(2,1)S(1)} collective-permute-done((bf16[128,1280]{1,0:T(8,128)(2,1)S(1)}, bf16[128,1280]{1,0:T(8,128)(2,1)S(1)}, u32[]{:S(2)}, u32[]{:S(2)}) %collective-permute-start.7) | collective-permute-done | bytes 327712 | tf_op jit(solution)/shard_map/ppermute | solution.py:48
  67.3 2.9 %collective-permute-start.9 = (bf16[16,768]{1,0:T(8,128)(2,1)S(1)}, bf16[16,768]{1,0:T(8,128)(2,1)S(1)}, u32[]{:S(2)}, u32[]{:S(2)}) collective-permute-start(bf16[16,768]{1,0:T(8,128)(2,1)S(1)} %slice.119), channel_id=1, source_target_pairs={{0,4},{4,8},{8,12},{12,16},{16,20},{20,24},{24,28},{1,5},{5,9},{9,... | collective-permute-start | bytes 73736 | tf_op jit(solution)/shard_map/ppermute | solution.py:21
  73.1 8.2 %mixer.1 = (bf16[512,256]{1,0:T(8,128)(2,1)}, f32[4,512,128]{2,1,0:T(8,128)}, f32[4,512,128]{2,1,0:T(8,128)}, f32[2,512]{1,0:T(2,128)}) custom-call(s32[2]{0:T(128)} %pad_add_fusion.where_ref, bf16[512,256]{1,0:T(8,128)(2,1)} %slice.117.pool_ref, bf16[512,512]{1,0:T(8,128)(2,1)} %get-tuple-element.26.value_ref, bf16[16,256]{1,0:T(8,128)(2,1)} %slice.120.edge_pool_ref, ...), custom_call_target="tpu_custom_call" | custom-call | tf_op jit(solution)/shard_map/mixer/pallas_call | solution.py:259
  81.3 3.9 %collective-permute-start.10 = (f32[2,512]{1,0:T(2,128)}, f32[2,512]{1,0:T(2,128)S(1)}, u32[]{:S(2)}, u32[]{:S(2)}) collective-permute-start(f32[2,512]{1,0:T(2,128)} %get-tuple-element.19), channel_id=1, source_target_pairs={{0,4},{4,8},{8,12},{12,16},{16,20},{20,24},{24,28},{1,5},{5,9},{9,... | collective-permute-start | bytes 12296 | tf_op jit(solution)/shard_map/ppermute | solution.py:21
  85.2 1.6 %collective-permute-start.14 = (bf16[256,768]{1,0:T(8,128)(2,1)S(1)}, bf16[256,768]{1,0:T(8,128)(2,1)S(1)}, u32[]{:S(2)}, u32[]{:S(2)}) collective-permute-start(bf16[256,768]{1,0:T(8,128)(2,1)S(1)} %pad_maximum_fusion.refs_0_), channel_id=1, source_target_pairs={{0,8},{8,16},{16,24},{24,28},{28,20},{20,12},{12,4},{4,0},{1,9},{9... | collective-permute-start | bytes 1179656 | tf_op jit(solution)/shard_map/ppermute | solution.py:48
  89.2 4.3 %collective-permute-start.11 = (f32[2,512]{1,0:T(2,128)S(1)}, f32[2,512]{1,0:T(2,128)S(1)}, u32[]{:S(2)}, u32[]{:S(2)}) collective-permute-start(f32[2,512]{1,0:T(2,128)S(1)} %maximum_select_fusion), channel_id=1, source_target_pairs={{0,8},{4,12},{8,16},{12,20},{16,24},{20,28},{1,9},{5,13},{9,17},{1... | collective-permute-start | bytes 12296 | tf_op jit(solution)/shard_map/ppermute | solution.py:21
  99.6 2.6 %collective-permute-start.12 = (f32[2,512]{1,0:T(2,128)S(1)}, f32[2,512]{1,0:T(2,128)S(1)}, u32[]{:S(2)}, u32[]{:S(2)}) collective-permute-start(f32[2,512]{1,0:T(2,128)S(1)} %maximum_select_fusion.1), channel_id=1, source_target_pairs={{0,16},{4,20},{8,24},{12,28},{1,17},{5,21},{9,25},{13,29},{2,18},{... | collective-permute-start | bytes 12296 | tf_op jit(solution)/shard_map/ppermute | solution.py:21
  102.3 4.2 %collective-permute-done.12 = f32[2,512]{1,0:T(2,128)S(1)} collective-permute-done((f32[2,512]{1,0:T(2,128)S(1)}, f32[2,512]{1,0:T(2,128)S(1)}, u32[]{:S(2)}, u32[]{:S(2)}) %collective-permute-start.12) | collective-permute-done | bytes 4128 | tf_op jit(solution)/shard_map/ppermute | solution.py:21
  106.4 2.3 %collective-permute-done.16.refs_3_ = bf16[256,768]{1,0:T(8,128)(2,1)S(1)} collective-permute-done((bf16[256,768]{1,0:T(8,128)(2,1)S(1)}, bf16[256,768]{1,0:T(8,128)(2,1)S(1)}, u32[]{:S(2)}, u32[]{:S(2)}) %collective-permute-start.16) | collective-permute-done | bytes 393248 | tf_op jit(solution)/shard_map/ppermute | solution.py:48
  108.9 1.9 %collective-permute-start.19 = (bf16[256,768]{1,0:T(8,128)(2,1)S(1)}, bf16[256,768]{1,0:T(8,128)(2,1)S(1)}, u32[]{:S(2)}, u32[]{:S(2)}) collective-permute-start(bf16[256,768]{1,0:T(8,128)(2,1)S(1)} %collective-permute-done.17.refs_4_), channel_id=1, source_target_pairs={{0,4},{8,0},{16,8},{24,16},{28,24},{20,28},{12,20},{4,12},{1,5},{9... | collective-permute-start | bytes 1179656 | tf_op jit(solution)/shard_map/ppermute | solution.py:49
  111.5 3.0 %collective-permute-start.13 = (f32[1,512]{1,0:T(1,128)S(1)}, f32[1,512]{1,0:T(1,128)S(1)}, u32[]{:S(2)}, u32[]{:S(2)}) collective-permute-start(f32[1,512]{1,0:T(1,128)S(1)} %slice_add_fusion), channel_id=1, source_target_pairs={{0,4},{4,8},{8,12},{12,16},{16,20},{20,24},{24,28},{1,5},{5,9},{9,... | collective-permute-start | bytes 6152 | tf_op jit(solution)/shard_map/ppermute | solution.py:21
  115.2 2.7 %collective-permute-done.18.refs_5_ = bf16[256,768]{1,0:T(8,128)(2,1)S(1)} collective-permute-done((bf16[256,768]{1,0:T(8,128)(2,1)S(1)}, bf16[256,768]{1,0:T(8,128)(2,1)S(1)}, u32[]{:S(2)}, u32[]{:S(2)}) %collective-permute-start.18) | collective-permute-done | bytes 393248 | tf_op jit(solution)/shard_map/ppermute | solution.py:48
  118.5 1.7 %collective-permute-start.21 = (bf16[128,768]{1,0:T(8,128)(2,1)S(1)}, bf16[128,768]{1,0:T(8,128)(2,1)S(1)}, u32[]{:S(2)}, u32[]{:S(2)}) collective-permute-start(bf16[128,768]{1,0:T(8,128)(2,1)S(1)} %slice.140), channel_id=1, source_target_pairs={{0,4},{8,0},{16,8},{24,16},{28,24},{20,28},{12,20},{4,12},{1,5},{9... | collective-permute-start | bytes 589832 | tf_op jit(solution)/shard_map/ppermute | solution.py:49
  120.8 2.8 %collective-permute-done.20.refs_7_ = bf16[128,768]{1,0:T(8,128)(2,1)S(1)} collective-permute-done((bf16[128,768]{1,0:T(8,128)(2,1)S(1)}, bf16[128,768]{1,0:T(8,128)(2,1)S(1)}, u32[]{:S(2)}, u32[]{:S(2)}) %collective-permute-start.20) | collective-permute-done | bytes 196640 | tf_op jit(solution)/shard_map/ppermute | solution.py:48
  125.8 5.3 %finish.1 = (bf16[512,512]{1,0:T(8,128)(2,1)}, bf16[256,2048]{1,0:T(8,128)(2,1)}) custom-call(s32[2]{0:T(128)} %pad_add_fusion.where_ref, s32[9]{0:T(128)} %stack.51.starts_ref, bf16[512,512]{1,0:T(8,128)(2,1)} %get-tuple-element.25.gate_ref, f32[4,512,128]{2,1,0:T(8,128)} %get-tuple-element.17.cum_ref, f32[4,512,128]{2,1,0:T(8,128)} %get-tuple-element.18.state_ref, ...), custom_call_target="tpu_custom_call" | custom-call | tf_op jit(solution)/shard_map/finish/pallas_call | solution.py:302
  131.1 4.5 %keep.1 = f32[256,2048]{1,0:T(8,128)} custom-call(s32[2]{0:T(128)} %pad_add_fusion.where_ref, s32[9]{0:T(128)} %stack.51.starts_ref, bf16[512,256]{1,0:T(8,128)(2,1)} %get-tuple-element.16.pool_ref, bf16[512,512]{1,0:T(8,128)(2,1)} %get-tuple-element.21.rnn_ref, bf16[256,768]{1,0:T(8,128)(2,1)} %copy-done.1, bf16[256,768]{1,0:T(8,128)(2,1)} %copy-done.4, ...), custom_call_target="tpu_custom_call" | custom-call | tf_op jit(solution)/shard_map/keep/pallas_call | solution.py:313
  135.6 2.8 %add_convert_fusion = bf16[256,2048]{1,0:T(8,128)(2,1)} fusion(f32[256,2048]{1,0:T(8,128)} %keep.1, bf16[256,2048]{1,0:T(8,128)(2,1)S(1)} %collective-permute-done.22), kind=kLoop, calls=%fused_computation.32 | loop fusion | flops 1572864 | bytes 4194304 | tf_op jit(solution)/shard_map/convert_element_type | solution.py:320
  (104 shorter events, 37.2 us)
Async XLA Ops:
  3.3 23.0 %collective-permute-start = (bf16[256,2048]{1,0:T(8,128)(2,1)S(1)}, bf16[256,2048]{1,0:T(8,128)(2,1)S(1)}, u32[]{:S(2)}, u32[]{:S(2)}) collective-permute-start(bf16[256,2048]{1,0:T(8,128)(2,1)S(1)} %fusion.8), channel_id=1, source_target_pairs={{0,1},{1,0},{2,3},{3,2},{4,5},{5,4},{6,7},{7,6},{8,9},{9,8},{10,11... | collective-permute-start | bytes 3145736 | tf_op jit(solution)/shard_map/ppermute | solution.py:229
  5.9 18.3 %collective-permute-start.2 = (bf16[256,1280]{1,0:T(8,128)(2,1)}, bf16[256,1280]{1,0:T(8,128)(2,1)}, u32[]{:S(2)}, u32[]{:S(2)}) collective-permute-start(bf16[256,1280]{1,0:T(8,128)(2,1)} %constant_dynamic-update-slice_fusion), channel_id=1, source_target_pairs={{0,4},{8,0},{16,8},{24,16},{28,24},{20,28},{12,20},{4,12},{1,5},{9... | collective-permute-start | bytes 1966088 | tf_op jit(solution)/shard_map/ppermute | solution.py:49
  8.5 17.4 %collective-permute-start.1 = (bf16[256,1280]{1,0:T(8,128)(2,1)}, bf16[256,1280]{1,0:T(8,128)(2,1)}, u32[]{:S(2)}, u32[]{:S(2)}) collective-permute-start(bf16[256,1280]{1,0:T(8,128)(2,1)} %constant_dynamic-update-slice_fusion), channel_id=1, source_target_pairs={{0,8},{8,16},{16,24},{24,28},{28,20},{20,12},{12,4},{4,0},{1,9},{9... | collective-permute-start | bytes 1966088 | tf_op jit(solution)/shard_map/ppermute | solution.py:48
  11.9 75.0 %copy-start.1 = (bf16[256,768]{1,0:T(8,128)(2,1)}, bf16[256,768]{1,0:T(8,128)(2,1)S(1)}, u32[]{:S(2)}) copy-start(bf16[256,768]{1,0:T(8,128)(2,1)S(1)} %pad_maximum_fusion.refs_0_) | copy-start | bytes 1179652
  24.2 18.5 %collective-permute-start.4 = (bf16[256,1280]{1,0:T(8,128)(2,1)}, bf16[256,1280]{1,0:T(8,128)(2,1)S(1)}, u32[]{:S(2)}, u32[]{:S(2)}) collective-permute-start(bf16[256,1280]{1,0:T(8,128)(2,1)} %collective-permute-done.2), channel_id=1, source_target_pairs={{0,4},{8,0},{16,8},{24,16},{28,24},{20,28},{12,20},{4,12},{1,5},{9... | collective-permute-start | bytes 1966088 | tf_op jit(solution)/shard_map/ppermute | solution.py:49
  25.9 16.2 %collective-permute-start.3 = (bf16[256,1280]{1,0:T(8,128)(2,1)}, bf16[256,1280]{1,0:T(8,128)(2,1)S(1)}, u32[]{:S(2)}, u32[]{:S(2)}) collective-permute-start(bf16[256,1280]{1,0:T(8,128)(2,1)} %collective-permute-done.1), channel_id=1, source_target_pairs={{0,8},{8,16},{16,24},{24,28},{28,20},{20,12},{12,4},{4,0},{1,9},{9... | collective-permute-start | bytes 1966088 | tf_op jit(solution)/shard_map/ppermute | solution.py:48
  42.1 15.1 %collective-permute-start.5 = (bf16[256,1280]{1,0:T(8,128)(2,1)S(1)}, bf16[256,1280]{1,0:T(8,128)(2,1)S(1)}, u32[]{:S(2)}, u32[]{:S(2)}) collective-permute-start(bf16[256,1280]{1,0:T(8,128)(2,1)S(1)} %collective-permute-done.3), channel_id=1, source_target_pairs={{0,8},{8,16},{16,24},{24,28},{28,20},{20,12},{12,4},{4,0},{1,9},{9... | collective-permute-start | bytes 1966088 | tf_op jit(solution)/shard_map/ppermute | solution.py:48
  42.7 15.5 %collective-permute-start.6 = (bf16[256,1280]{1,0:T(8,128)(2,1)S(1)}, bf16[256,1280]{1,0:T(8,128)(2,1)S(1)}, u32[]{:S(2)}, u32[]{:S(2)}) collective-permute-start(bf16[256,1280]{1,0:T(8,128)(2,1)S(1)} %collective-permute-done.4), channel_id=1, source_target_pairs={{0,4},{8,0},{16,8},{24,16},{28,24},{20,28},{12,20},{4,12},{1,5},{9... | collective-permute-start | bytes 1966088 | tf_op jit(solution)/shard_map/ppermute | solution.py:49
  57.3 7.3 %collective-permute-start.7 = (bf16[128,1280]{1,0:T(8,128)(2,1)S(1)}, bf16[128,1280]{1,0:T(8,128)(2,1)S(1)}, u32[]{:S(2)}, u32[]{:S(2)}) collective-permute-start(bf16[128,1280]{1,0:T(8,128)(2,1)S(1)} %slice.115), channel_id=1, source_target_pairs={{0,8},{8,16},{16,24},{24,28},{28,20},{20,12},{12,4},{4,0},{1,9},{9... | collective-permute-start | bytes 983048 | tf_op jit(solution)/shard_map/ppermute | solution.py:48
  58.3 7.3 %collective-permute-start.8 = (bf16[128,1280]{1,0:T(8,128)(2,1)S(1)}, bf16[128,1280]{1,0:T(8,128)(2,1)S(1)}, u32[]{:S(2)}, u32[]{:S(2)}) collective-permute-start(bf16[128,1280]{1,0:T(8,128)(2,1)S(1)} %slice.116), channel_id=1, source_target_pairs={{0,4},{8,0},{16,8},{24,16},{28,24},{20,28},{12,20},{4,12},{1,5},{9... | collective-permute-start | bytes 983048 | tf_op jit(solution)/shard_map/ppermute | solution.py:49
  67.3 4.7 %collective-permute-start.9 = (bf16[16,768]{1,0:T(8,128)(2,1)S(1)}, bf16[16,768]{1,0:T(8,128)(2,1)S(1)}, u32[]{:S(2)}, u32[]{:S(2)}) collective-permute-start(bf16[16,768]{1,0:T(8,128)(2,1)S(1)} %slice.119), channel_id=1, source_target_pairs={{0,4},{4,8},{8,12},{12,16},{16,20},{20,24},{24,28},{1,5},{5,9},{9,... | collective-permute-start | bytes 73736 | tf_op jit(solution)/shard_map/ppermute | solution.py:21
  81.3 6.5 %collective-permute-start.10 = (f32[2,512]{1,0:T(2,128)}, f32[2,512]{1,0:T(2,128)S(1)}, u32[]{:S(2)}, u32[]{:S(2)}) collective-permute-start(f32[2,512]{1,0:T(2,128)} %get-tuple-element.19), channel_id=1, source_target_pairs={{0,4},{4,8},{8,12},{12,16},{16,20},{20,24},{24,28},{1,5},{5,9},{9,... | collective-permute-start | bytes 12296 | tf_op jit(solution)/shard_map/ppermute | solution.py:21
  85.2 10.8 %collective-permute-start.14 = (bf16[256,768]{1,0:T(8,128)(2,1)S(1)}, bf16[256,768]{1,0:T(8,128)(2,1)S(1)}, u32[]{:S(2)}, u32[]{:S(2)}) collective-permute-start(bf16[256,768]{1,0:T(8,128)(2,1)S(1)} %pad_maximum_fusion.refs_0_), channel_id=1, source_target_pairs={{0,8},{8,16},{16,24},{24,28},{28,20},{20,12},{12,4},{4,0},{1,9},{9... | collective-permute-start | bytes 1179656 | tf_op jit(solution)/shard_map/ppermute | solution.py:48
  86.9 10.4 %collective-permute-start.15 = (bf16[256,768]{1,0:T(8,128)(2,1)S(1)}, bf16[256,768]{1,0:T(8,128)(2,1)S(1)}, u32[]{:S(2)}, u32[]{:S(2)}) collective-permute-start(bf16[256,768]{1,0:T(8,128)(2,1)S(1)} %pad_maximum_fusion.refs_0_), channel_id=1, source_target_pairs={{0,4},{8,0},{16,8},{24,16},{28,24},{20,28},{12,20},{4,12},{1,5},{9... | collective-permute-start | bytes 1179656 | tf_op jit(solution)/shard_map/ppermute | solution.py:49
  89.2 5.6 %collective-permute-start.11 = (f32[2,512]{1,0:T(2,128)S(1)}, f32[2,512]{1,0:T(2,128)S(1)}, u32[]{:S(2)}, u32[]{:S(2)}) collective-permute-start(f32[2,512]{1,0:T(2,128)S(1)} %maximum_select_fusion), channel_id=1, source_target_pairs={{0,8},{4,12},{8,16},{12,20},{16,24},{20,28},{1,9},{5,13},{9,17},{1... | collective-permute-start | bytes 12296 | tf_op jit(solution)/shard_map/ppermute | solution.py:21
  96.0 12.8 %collective-permute-start.16 = (bf16[256,768]{1,0:T(8,128)(2,1)S(1)}, bf16[256,768]{1,0:T(8,128)(2,1)S(1)}, u32[]{:S(2)}, u32[]{:S(2)}) collective-permute-start(bf16[256,768]{1,0:T(8,128)(2,1)S(1)} %collective-permute-done.14.refs_1_), channel_id=1, source_target_pairs={{0,8},{8,16},{16,24},{24,28},{28,20},{20,12},{12,4},{4,0},{1,9},{9... | collective-permute-start | bytes 1179656 | tf_op jit(solution)/shard_map/ppermute | solution.py:48
  97.3 11.6 %collective-permute-start.17 = (bf16[256,768]{1,0:T(8,128)(2,1)S(1)}, bf16[256,768]{1,0:T(8,128)(2,1)S(1)}, u32[]{:S(2)}, u32[]{:S(2)}) collective-permute-start(bf16[256,768]{1,0:T(8,128)(2,1)S(1)} %collective-permute-done.15.refs_2_), channel_id=1, source_target_pairs={{0,4},{8,0},{16,8},{24,16},{28,24},{20,28},{12,20},{4,12},{1,5},{9... | collective-permute-start | bytes 1179656 | tf_op jit(solution)/shard_map/ppermute | solution.py:49
  99.6 6.8 %collective-permute-start.12 = (f32[2,512]{1,0:T(2,128)S(1)}, f32[2,512]{1,0:T(2,128)S(1)}, u32[]{:S(2)}, u32[]{:S(2)}) collective-permute-start(f32[2,512]{1,0:T(2,128)S(1)} %maximum_select_fusion.1), channel_id=1, source_target_pairs={{0,16},{4,20},{8,24},{12,28},{1,17},{5,21},{9,25},{13,29},{2,18},{... | collective-permute-start | bytes 12296 | tf_op jit(solution)/shard_map/ppermute | solution.py:21
  108.8 9.1 %collective-permute-start.18 = (bf16[256,768]{1,0:T(8,128)(2,1)S(1)}, bf16[256,768]{1,0:T(8,128)(2,1)S(1)}, u32[]{:S(2)}, u32[]{:S(2)}) collective-permute-start(bf16[256,768]{1,0:T(8,128)(2,1)S(1)} %collective-permute-done.16.refs_3_), channel_id=1, source_target_pairs={{0,8},{8,16},{16,24},{24,28},{28,20},{20,12},{12,4},{4,0},{1,9},{9... | collective-permute-start | bytes 1179656 | tf_op jit(solution)/shard_map/ppermute | solution.py:48
  108.9 9.6 %collective-permute-start.19 = (bf16[256,768]{1,0:T(8,128)(2,1)S(1)}, bf16[256,768]{1,0:T(8,128)(2,1)S(1)}, u32[]{:S(2)}, u32[]{:S(2)}) collective-permute-start(bf16[256,768]{1,0:T(8,128)(2,1)S(1)} %collective-permute-done.17.refs_4_), channel_id=1, source_target_pairs={{0,4},{8,0},{16,8},{24,16},{28,24},{20,28},{12,20},{4,12},{1,5},{9... | collective-permute-start | bytes 1179656 | tf_op jit(solution)/shard_map/ppermute | solution.py:49
  111.5 8.7 %collective-permute-start.13 = (f32[1,512]{1,0:T(1,128)S(1)}, f32[1,512]{1,0:T(1,128)S(1)}, u32[]{:S(2)}, u32[]{:S(2)}) collective-permute-start(f32[1,512]{1,0:T(1,128)S(1)} %slice_add_fusion), channel_id=1, source_target_pairs={{0,4},{4,8},{8,12},{12,16},{16,20},{20,24},{24,28},{1,5},{5,9},{9,... | collective-permute-start | bytes 6152 | tf_op jit(solution)/shard_map/ppermute | solution.py:21
  117.9 5.7 %collective-permute-start.20 = (bf16[128,768]{1,0:T(8,128)(2,1)S(1)}, bf16[128,768]{1,0:T(8,128)(2,1)S(1)}, u32[]{:S(2)}, u32[]{:S(2)}) collective-permute-start(bf16[128,768]{1,0:T(8,128)(2,1)S(1)} %slice.139), channel_id=1, source_target_pairs={{0,8},{8,16},{16,24},{24,28},{28,20},{20,12},{12,4},{4,0},{1,9},{9... | collective-permute-start | bytes 589832 | tf_op jit(solution)/shard_map/ppermute | solution.py:48
  118.5 6.6 %collective-permute-start.21 = (bf16[128,768]{1,0:T(8,128)(2,1)S(1)}, bf16[128,768]{1,0:T(8,128)(2,1)S(1)}, u32[]{:S(2)}, u32[]{:S(2)}) collective-permute-start(bf16[128,768]{1,0:T(8,128)(2,1)S(1)} %slice.140), channel_id=1, source_target_pairs={{0,4},{8,0},{16,8},{24,16},{28,24},{20,28},{12,20},{4,12},{1,5},{9... | collective-permute-start | bytes 589832 | tf_op jit(solution)/shard_map/ppermute | solution.py:49
  131.1 4.6 %collective-permute-start.22 = (bf16[256,2048]{1,0:T(8,128)(2,1)}, bf16[256,2048]{1,0:T(8,128)(2,1)S(1)}, u32[]{:S(2)}, u32[]{:S(2)}) collective-permute-start(bf16[256,2048]{1,0:T(8,128)(2,1)} %get-tuple-element.22), channel_id=1, source_target_pairs={{0,1},{1,0},{2,3},{3,2},{4,5},{5,4},{6,7},{7,6},{8,9},{9,8},{10,11... | collective-permute-start | bytes 3145736 | tf_op jit(solution)/shard_map/ppermute | solution.py:312
  (18 other events, 241.9 us)
